TPU v7x, 512 devices: a whole 4x8x8 slice. The times are simulated.
512 devices in a mesh: ep: 32 (over z, x), tp: 16 (over y, core).
Axes of the slice: x: 4, y: 8, z: 8, core: 2. Of those that a mesh axis runs over, the one named last changes fastest.
Arguments:
- query_rows: bfloat16 [16384, 3072], P('ep', 'tp'), may hold values from -6 to 6
- key_rows: bfloat16 [16384, 1024], P('ep', 'tp'), may hold values from -6 to 6
- value_rows: bfloat16 [16384, 1024], P('ep', 'tp'), may hold values from -6 to 6
- query_gain: float32 [48, 64], P('tp'), may hold values from 0.4 to 48
- key_gain: float32 [16, 64], P('tp'), may hold values from 0.1 to 1.9
- sink_logits: float32 [48], P('tp'), may hold values from 1 to 6
- out_weight: bfloat16 [3072, 2048], P('tp'), may hold values from -0.109375 to 0.109375
- expert_input: bfloat16 [16384, 2048], P(('ep', 'tp')), may hold values from -6 to 6
- expert_gain: float32 [2048], replicated, may hold values from 0.1 to 1.9
- routes: int32 [16384, 2], P(('ep', 'tp')), may hold values from 0 to 31, all different within a row; in each aligned block of 32 rows (0 to 31, 32 to 63, ...) at most 3 rows name the same one
- route_logits: float32 [16384, 2], P(('ep', 'tp')), may hold values from -6 to 6
- gate_weight: bfloat16 [32, 2048, 2048], P('ep', None, 'tp'), may hold values from -0.375 to 0.375
- up_weight: bfloat16 [32, 2048, 2048], P('ep', None, 'tp'), may hold values from -0.375 to 0.375
- down_weight: bfloat16 [32, 2048, 2048], P('ep', 'tp'), may hold values from -0.01953125 to 0.01953125
Outputs:
- attended: bfloat16 [16384, 2048], P(('ep', 'tp'))
- expert_mix: bfloat16 [16384, 2048], P(('ep', 'tp'))
Inputs may be any that keep to these rules, and one draw needn't show every extreme that they name: `routes`: each row names 2 different experts; in the rows of one device no expert is named more than 3 times, and in some device one expert is named exactly 3 times.
All inputs are finite; a program needn't handle non-finite values.
Results may differ from a plain program's by a relative error of at most 0.017.
The roundings to bfloat16 on the way count: a program that leaves them out, or rounds other values in their place, can miss the bound.
Values may be sent and summed in bfloat16 or wider, within the bound.
A program may use at most 64 MiB of HBM per device.

v0:
```python
import jax
import jax.numpy as jnp
from jax import lax
from jax.sharding import PartitionSpec as P

EXPERTS = 32
WINDOW = 128


EPSILON = 1e-06
CLAMP_LIMIT = 7.0
ACT_SLOPE = 1.702
NEGATIVE = -1e30


def shifted(value, axis, steps):
    count = lax.axis_size(axis)
    initial, last = (max(0, -steps), min(count, count - steps))
    return lax.ppermute(value, axis, [(source, source + steps) for source in range(initial, last)])


def head_norm(row_data, gain_table):
    head_count, head_size = gain_table.shape
    widened = row_data.astype(jnp.float32).reshape(row_data.shape[0], head_count, head_size)
    scaled = widened * lax.rsqrt(jnp.mean(widened * widened, axis=-1, keepdims=True) + EPSILON)
    return (scaled * gain_table).astype(jnp.bfloat16)


def band(padded, blocks):
    tiled = padded.reshape((blocks + 1, WINDOW) + padded.shape[1:])
    return jnp.concatenate([tiled[:-1], tiled[1:]], axis=1)


def attend(query_rows, key_rows, value_rows, query_gain, key_gain, sink_logits):
    seq_rows = query_rows.shape[0]
    key_heads, head_size = key_gain.shape
    group_size = query_gain.shape[0] // key_heads
    blocks = seq_rows // WINDOW
    query_hat = head_norm(query_rows, query_gain).reshape(
        blocks, WINDOW, key_heads, group_size, head_size
    )
    key_hat = head_norm(key_rows, key_gain)
    value_hat = value_rows.reshape(seq_rows, key_heads, head_size)
    tail_rows = jnp.stack([key_hat[seq_rows - WINDOW :], value_hat[seq_rows - WINDOW :]])
    earlier = shifted(tail_rows, "ep", 1)
    key_band = band(jnp.concatenate([earlier[0], key_hat], axis=0), blocks)
    value_band = band(jnp.concatenate([earlier[1], value_hat], axis=0), blocks)
    query_pos = lax.broadcasted_iota(jnp.int32, (WINDOW, 2 * WINDOW), 0)
    key_pos = lax.broadcasted_iota(jnp.int32, (WINDOW, 2 * WINDOW), 1)
    distance = query_pos + WINDOW - key_pos
    inside = (distance >= 0) & (distance < WINDOW)
    first_block = (lax.broadcasted_iota(jnp.int32, (blocks, 1, 1), 0) == 0) & (
        lax.axis_index("ep") == 0
    )
    allowed = inside[None] & ~(first_block & (key_pos < WINDOW)[None])
    scores = jnp.einsum(
        "bqkgd,bjkd->bkgqj", query_hat, key_band, preferred_element_type=jnp.float32
    ) * head_size ** (-0.5)
    scores = jnp.where(allowed[:, None, None], scores, NEGATIVE)
    sink_table = sink_logits.reshape(1, key_heads, group_size, 1, 1)
    highest = jnp.maximum(jnp.max(scores, axis=-1, keepdims=True), sink_table)
    weights = jnp.exp(scores - highest)
    total = jnp.sum(weights, axis=-1, keepdims=True) + jnp.exp(sink_table - highest)
    mixed = jnp.einsum(
        "bkgqj,bjkd->bkgqd",
        weights.astype(jnp.bfloat16),
        value_band,
        preferred_element_type=jnp.float32,
    )
    mixed = (mixed / total).astype(jnp.bfloat16)
    return jnp.transpose(mixed, (0, 3, 1, 2, 4)).reshape(seq_rows, -1)


def slot_maps(route_block, capacity):
    flat_routes = route_block.reshape(-1)
    expert_hot = (flat_routes[:, None] == lax.broadcasted_iota(jnp.int32, (1, EXPERTS), 1)).astype(
        jnp.int32
    )
    before = jnp.cumsum(expert_hot, axis=0) - expert_hot
    position = jnp.sum(before * expert_hot, axis=1)
    place_hot = (position[:, None] == lax.broadcasted_iota(jnp.int32, (1, capacity), 1)).astype(
        jnp.float32
    )
    row_total, fanout = route_block.shape
    return (
        expert_hot.astype(jnp.float32).reshape(row_total, fanout, EXPERTS),
        place_hot.reshape(row_total, fanout, capacity),
    )


def dispatch_matrix(route_block, capacity):
    expert_hot, place_hot = slot_maps(route_block, capacity)
    return jnp.einsum("rke,rkc->ecr", expert_hot, place_hot).astype(jnp.bfloat16)


def combine_matrix(route_block, route_weight, capacity):
    expert_hot, place_hot = slot_maps(route_block, capacity)
    return jnp.einsum("rke,rkc,rk->rec", expert_hot, place_hot, route_weight)


def expert_hidden(piece, gate_weight, up_weight):
    gate_pre = jnp.einsum("aecd,edf->aecf", piece, gate_weight, preferred_element_type=jnp.float32)
    up_pre = jnp.einsum("aecd,edf->aecf", piece, up_weight, preferred_element_type=jnp.float32)
    clipped = jnp.minimum(gate_pre, CLAMP_LIMIT)
    linear = jnp.clip(up_pre, -CLAMP_LIMIT, CLAMP_LIMIT)
    return (clipped * jax.nn.sigmoid(ACT_SLOPE * clipped) * (linear + 1.0)).astype(jnp.bfloat16)


def on_device(
    query_rows,
    key_rows,
    value_rows,
    query_gain,
    key_gain,
    sink_logits,
    out_weight,
    expert_input,
    expert_gain,
    routes,
    route_logits,
    gate_weight,
    up_weight,
    down_weight,
):
    heads_out = attend(query_rows, key_rows, value_rows, query_gain, key_gain, sink_logits)
    attended = lax.psum_scatter(
        jnp.dot(heads_out, out_weight, preferred_element_type=jnp.float32).astype(jnp.bfloat16),
        "tp",
        scatter_dimension=0,
        tiled=True,
    )
    own_rows = expert_input.shape[0]
    fanout = routes.shape[1]
    capacity = (3 * own_rows * fanout + 2 * EXPERTS - 1) // (2 * EXPERTS)
    ep_size = lax.axis_size("ep")
    tp_size = lax.axis_size("tp")
    local_experts = gate_weight.shape[0]
    widened = expert_input.astype(jnp.float32)
    normed = (
        widened
        * lax.rsqrt(jnp.mean(widened * widened, axis=-1, keepdims=True) + EPSILON)
        * expert_gain
    ).astype(jnp.bfloat16)
    route_weight = jax.nn.softmax(route_logits, axis=-1)
    combine = combine_matrix(routes, route_weight, capacity)
    sender = dispatch_matrix(routes, capacity)
    slot_rows = jnp.einsum(
        "ecr,rd->ecd", sender, normed, preferred_element_type=jnp.float32
    ).astype(jnp.bfloat16)
    slot_rows = slot_rows.reshape(ep_size, local_experts, capacity, -1)
    arrived = lax.all_to_all(slot_rows, "ep", split_axis=0, concat_axis=0, tiled=True)
    hidden_units = expert_hidden(
        lax.all_gather(arrived, "tp", axis=0, tiled=True), gate_weight, up_weight
    )
    partial_value = jnp.einsum(
        "aecf,efd->aecd", hidden_units, down_weight, preferred_element_type=jnp.float32
    ).astype(jnp.bfloat16)
    partial_value = partial_value.reshape(tp_size, ep_size * local_experts * capacity, -1)
    pieces = lax.all_to_all(partial_value, "tp", split_axis=0, concat_axis=0, tiled=True)
    summed = jnp.sum(pieces, axis=0, dtype=jnp.float32).astype(jnp.bfloat16)
    summed = summed.reshape(ep_size, local_experts * capacity, -1)
    returned = lax.all_to_all(summed, "ep", split_axis=0, concat_axis=0, tiled=True)
    expert_mix = jnp.einsum("rec,ecd->rd", combine, returned.astype(jnp.float32)).astype(
        jnp.bfloat16
    )
    return (attended, expert_mix)


def solution(mesh):
    placed = (
        P("ep", "tp"),
        P("ep", "tp"),
        P("ep", "tp"),
        P("tp", None),
        P("tp", None),
        P("tp"),
        P("tp", None),
        P(("ep", "tp"), None),
        P(),
        P(("ep", "tp"), None),
        P(("ep", "tp"), None),
        P("ep", None, "tp"),
        P("ep", None, "tp"),
        P("ep", "tp", None),
    )
    return jax.shard_map(
        on_device,
        mesh=mesh,
        in_specs=placed,
        out_specs=(P(("ep", "tp"), None), P(("ep", "tp"), None)),
        check_vma=False,
    )
```

profile of v0, /device:TPU:24, one launch (start us, length us, event | category | flops | bytes accessed | tf_op | source)
XLA Modules:
  0.0 328.0 jit_solution(9556012948772609825)
XLA Ops:
  7.2 1.1 fusion.58
  8.3 0.8 copy.42
  9.7 0.4 fusion.34
  10.1 1.2 fusion.4
  11.6 30.7 %all_to_all.15 = bf16[32,1,3,2048]{3,2,1,0:T(4,128)(2,1)S(1)} all-to-all(bf16[32,1,3,2048]{3,2,1,0:T(4,128)(2,1)S(1)} %copy.46), channel_id=1, replica_groups=mesh['ep'=32,'tp'=16] {'ep'}, dimensions={0} | all-to-all | bytes 786432 | tf_op jit(solution)/shard_map/all_to_all | solution.py:151
  42.3 1.1 copy.47
  43.5 44.1 %all-gather.2.cloned.1.call-done = bf16[512,1,3,2048]{3,0,2,1:T(8,128)(2,1)} async-done(((bf16[32,1,3,2048]{3,0,2,1:T(8,128)(2,1)}), bf16[512,1,3,2048]{3,0,2,1:T(8,128)(2,1)}) %all-gather.2.cloned.1.call-update) | async-done | bytes 6291472 | tf_op jit(solution)/shard_map/all_gather | solution.py:153
  87.5 4.6 %fusion.11 = f32[512,1,3,128]{3,0,2,1:T(8,128)S(1)} fusion(bf16[512,1,3,2048]{3,0,2,1:T(8,128)(2,1)} %all-gather.2.cloned.1.call-done, bf16[1,2048,128]{2,1,0:T(8,128)(2,1)S(1)} %copy-done.9), kind=kOutput, calls=%fused_computation.15 | convolution fusion | flops 805502976 | bytes 7602176 | tf_op jit(solution)/shard_map/aecd,edf->aecf/dot_general | solution.py:102
  92.1 11.9 %convert_bitcast_fusion = bf16[512,1,3,2048]{3,0,2,1:T(8,128)(2,1)} fusion(bf16[512,1,3,2048]{3,0,2,1:T(8,128)(2,1)} %all-gather.2.cloned.1.call-done, f32[512,1,3,128]{3,0,2,1:T(8,128)S(1)} %fusion.11, bf16[1,128,2048]{2,1,0:T(8,128)(2,1)S(1)} %copy-done.3, bf16[1,2048,128]{2,1,0:T(8,128)(2,1)S(1)} %copy-done.4), kind=kOutput, calls=%fused_computation.4 | convolution fusion | flops 1615527936 | bytes 14417920 | tf_op jit(solution)/shard_map/aecf,efd->aecd/dot_general | solution.py:155
  104.1 11.6 %copy.48 = bf16[512,1,3,2048]{3,2,0,1:T(4,128)(2,1)} copy(bf16[512,1,3,2048]{3,0,2,1:T(8,128)(2,1)} %convert_bitcast_fusion) | data formatting | bytes 12582912 | tf_op jit(solution)/shard_map/convert_element_type | solution.py:157
  115.6 16.3 %reshape.224 = bf16[16,96,2048]{2,1,0:T(8,128)(2,1)} reshape(bf16[512,1,3,2048]{3,2,0,1:T(4,128)(2,1)} %copy.48) | data formatting | bytes 12582912 | tf_op jit(solution)/shard_map/reshape | solution.py:158
  132.0 5.5 %all-to-all-start.1 = ((bf16[16,96,2048]{2,1,0:T(8,128)(2,1)}), bf16[16,96,2048]{2,1,0:T(8,128)(2,1)}, u32[]{:S(2)}, u32[]{:S(2)}) async-start(bf16[16,96,2048]{2,1,0:T(8,128)(2,1)} %reshape.224), calls=%async_computation.2 | async-start | bytes 12582912 | tf_op jit(solution)/shard_map/all_to_all | solution.py:159
  137.7 3.4 %collective-permute-start = (bf16[2,128,1,64]{1,3,2,0:T(8,128)(2,1)S(1)}, bf16[2,128,1,64]{1,3,2,0:T(8,128)(2,1)S(1)}, u32[]{:S(2)}, u32[]{:S(2)}) collective-permute-start(bf16[2,128,1,64]{1,3,2,0:T(8,128)(2,1)S(1)} %pad_maximum_fusion.2), channel_id=1, source_target_pairs={{0,16},{16,32},{32,48},{48,64},{64,80},{80,96},{96,112},{112,128},... | collective-permute-start | bytes 98312 | tf_op jit(solution)/shard_map/ppermute | solution.py:19
  141.8 0.9 collective-permute-done
  142.7 0.5 fusion.105
  143.6 0.4 fusion.33
  144.1 2.1 convolution_convert_fusion
  146.3 140.4 %all-to-all-done.1 = bf16[16,96,2048]{2,1,0:T(8,128)(2,1)} async-done(((bf16[16,96,2048]{2,1,0:T(8,128)(2,1)}), bf16[16,96,2048]{2,1,0:T(8,128)(2,1)}, u32[]{:S(2)}, u32[]{:S(2)}) %all-to-all-start.1) | async-done | bytes 6291488 | tf_op jit(solution)/shard_map/all_to_all | solution.py:159
  286.7 4.1 %reduce_sum.76 = bf16[96,2048]{1,0:T(8,128)(2,1)S(1)} reduce(bf16[16,96,2048]{2,1,0:T(8,128)(2,1)} %all-to-all-done.1, bf16[]{:T(256)} %constant.49.clone.1), dimensions={0}, to_apply=%region_10.11 | reduce | flops 2949120 | bytes 6684674 | tf_op jit(solution)/shard_map/reduce_sum | solution.py:160
  290.8 1.0 reshape.225
  291.8 10.2 %all-to-all-start.2 = ((bf16[32,3,2048]{2,1,0:T(4,128)(2,1)}), bf16[32,3,2048]{2,1,0:T(4,128)(2,1)S(1)}, u32[]{:S(2)}, u32[]{:S(2)}) async-start(bf16[32,3,2048]{2,1,0:T(4,128)(2,1)} %reshape.225), calls=%async_computation.3 | async-start | bytes 1048576 | tf_op jit(solution)/shard_map/all_to_all | solution.py:162
  302.2 0.4 fusion.84
  302.5 17.5 %all-to-all-done.2 = bf16[32,3,2048]{2,1,0:T(4,128)(2,1)S(1)} async-done(((bf16[32,3,2048]{2,1,0:T(4,128)(2,1)}), bf16[32,3,2048]{2,1,0:T(4,128)(2,1)S(1)}, u32[]{:S(2)}, u32[]{:S(2)}) %all-to-all-start.2) | async-done | bytes 393248 | tf_op jit(solution)/shard_map/all_to_all | solution.py:162
  320.1 1.1 fusion.5
  (64 shorter events, 2.5 us)
Async XLA Ops:
  7.2 137.0 %copy-start = (bf16[192,2048]{1,0:T(8,128)(2,1)S(1)}, bf16[192,2048]{1,0:T(8,128)(2,1)}, u32[]{:S(2)}) copy-start(bf16[192,2048]{1,0:T(8,128)(2,1)} %param.20) | copy-start | bytes 2359300
  7.2 80.4 %all-gather.2.cloned.1.call-start = ((), (), s32[]{:S(2)}) async-start(), calls=%async_computation.5 | async-start | bytes 6684672 | tf_op jit(solution)/shard_map/all_gather | solution.py:153
  9.7 77.9 %copy-start.9 = (bf16[1,2048,128]{2,1,0:T(8,128)(2,1)S(1)}, bf16[1,2048,128]{2,1,0:T(8,128)(2,1)}, u32[]{:S(2)}) copy-start(bf16[1,2048,128]{2,1,0:T(8,128)(2,1)} %param.25) | copy-start | bytes 1572868
  43.4 48.7 %copy-start.3 = (bf16[1,128,2048]{2,1,0:T(8,128)(2,1)S(1)}, bf16[1,128,2048]{2,1,0:T(8,128)(2,1)}, u32[]{:S(2)}) copy-start(bf16[1,128,2048]{2,1,0:T(8,128)(2,1)} %param.27) | copy-start | bytes 1572868
  43.4 48.7 %copy-start.4 = (bf16[1,2048,128]{2,1,0:T(8,128)(2,1)S(1)}, bf16[1,2048,128]{2,1,0:T(8,128)(2,1)}, u32[]{:S(2)}) copy-start(bf16[1,2048,128]{2,1,0:T(8,128)(2,1)} %param.26) | copy-start | bytes 1572868
  131.9 5.6 %copy-start.2 = (bf16[512,64]{0,1:T(8,128)(2,1)S(1)}, bf16[512,64]{0,1:T(8,128)(2,1)}, u32[]{:S(2)}) copy-start(bf16[512,64]{0,1:T(8,128)(2,1)} %param.15) | copy-start | bytes 196612
  132.0 5.6 %copy-start.7 = (f32[1,64]{1,0:T(1,128)S(1)}, f32[1,64]{1,0:T(1,128)}, u32[]{:S(2)}) copy-start(f32[1,64]{1,0:T(1,128)} %param.18) | copy-start | bytes 772
  132.0 5.7 %copy-start.5 = (bf16[512,64]{0,1:T(8,128)(2,1)S(1)}, bf16[512,64]{0,1:T(8,128)(2,1)}, u32[]{:S(2)}) copy-start(bf16[512,64]{0,1:T(8,128)(2,1)} %param.16) | copy-start | bytes 196612
  132.0 9.1 %copy-start.1 = (bf16[512,192]{0,1:T(8,128)(2,1)S(1)}, bf16[512,192]{0,1:T(8,128)(2,1)}, u32[]{:S(2)}) copy-start(bf16[512,192]{0,1:T(8,128)(2,1)} %param.14) | copy-start | bytes 589828
  132.0 154.7 %all-to-all-start.1 = ((bf16[16,96,2048]{2,1,0:T(8,128)(2,1)}), bf16[16,96,2048]{2,1,0:T(8,128)(2,1)}, u32[]{:S(2)}, u32[]{:S(2)}) async-start(bf16[16,96,2048]{2,1,0:T(8,128)(2,1)} %reshape.224), calls=%async_computation.2 | async-start | bytes 12582912 | tf_op jit(solution)/shard_map/all_to_all | solution.py:159
  137.5 5.3 %copy-start.10 = (f32[3,64]{1,0:T(4,128)S(1)}, f32[3,64]{1,0:T(4,128)}, u32[]{:S(2)}) copy-start(f32[3,64]{1,0:T(4,128)} %param.17) | copy-start | bytes 2308
  137.5 183.7 %reduce-scatter.2.cloned.1.call-start = ((), (), s32[]{:S(2)}) async-start(), calls=%async_computation.4 | async-start | bytes 2228224 | tf_op jit(solution)/shard_map/reduce_scatter | solution.py:126
  137.7 5.0 %collective-permute-start = (bf16[2,128,1,64]{1,3,2,0:T(8,128)(2,1)S(1)}, bf16[2,128,1,64]{1,3,2,0:T(8,128)(2,1)S(1)}, u32[]{:S(2)}, u32[]{:S(2)}) collective-permute-start(bf16[2,128,1,64]{1,3,2,0:T(8,128)(2,1)S(1)} %pad_maximum_fusion.2), channel_id=1, source_target_pairs={{0,16},{16,32},{32,48},{48,64},{64,80},{80,96},{96,112},{112,128},... | collective-permute-start | bytes 98312 | tf_op jit(solution)/shard_map/ppermute | solution.py:19
  141.2 2.0 copy-start.8
  146.3 155.7 %copy-start.6 = (f32[32,2]{0,1:T(2,128)S(1)}, f32[32,2]{0,1:T(2,128)}, u32[]{:S(2)}) copy-start(f32[32,2]{0,1:T(2,128)} %param.24) | copy-start | bytes 772
  291.8 28.3 %all-to-all-start.2 = ((bf16[32,3,2048]{2,1,0:T(4,128)(2,1)}), bf16[32,3,2048]{2,1,0:T(4,128)(2,1)S(1)}, u32[]{:S(2)}, u32[]{:S(2)}) async-start(bf16[32,3,2048]{2,1,0:T(4,128)(2,1)} %reshape.225), calls=%async_computation.3 | async-start | bytes 1048576 | tf_op jit(solution)/shard_map/all_to_all | solution.py:162
Sparse Core Ops, SparseCore 0:
  43.6 43.9 all-gather.1
  146.4 136.6 reduce-scatter.1
where the time goes:
time: 329 us; the launch traced here: 328 us
  waiting for transfers between devices  203 us (62%)
  local copies, waits for them, and re-layouts  31.8 us (10%)
  blocking collectives  30.7 us (9%)
  matrix products  22.5 us (7%)
  starting transfers between devices  19.1 us (6%)
  between operations  14.4 us (4%)
  other arithmetic  6.53 us (2%)
    all_to_all x1, waiting for transfers between devices, on_device(): lax.all_to_all(partial_value, 'tp', split_axis=0, concat_axis=0, tiled=True)  140 us
    all_gather x1, waiting for transfers between devices, on_device(): lax.all_gather(arrived, 'tp', axis=0, tiled=True)  44.1 us
    all_to_all x1, blocking collectives, on_device(): lax.all_to_all(slot_rows, 'ep', split_axis=0, concat_axis=0, tiled=True)  30.7 us
    all_to_all x1, waiting for transfers between devices, on_device(): lax.all_to_all(summed, 'ep', split_axis=0, concat_axis=0, tiled=True)  17.5 us
    reshape x1, local copies, waits for them, and re-layouts, on_device(): partial_value.reshape(tp_size, ep_size * local_experts * capacity, -1)  16.3 us
    dot_general x1, matrix products, on_device(): jnp.einsum('aecf,efd->aecd', hidden_units, down_weight, preferred_element...  11.9 us
    convert_element_type x1, local copies, waits for them, and re-layouts, on_device(): partial_value = jnp.einsum('aecf,efd->aecd', hidden_units, down_weight, p...  11.6 us
    all_to_all x1, starting transfers between devices, on_device(): lax.all_to_all(summed, 'ep', split_axis=0, concat_axis=0, tiled=True)  10.2 us
  transfers between devices with their start and end apart: 5, of which 4 were waited for; matrix products, arithmetic and copies ran while one was open for 3% of the time, Pallas kernels for 0%

commit v1 on v0

--- a/solution.py
+++ b/solution.py
@@ -1,6 +1,8 @@
 import jax
 import jax.numpy as jnp
 from jax import lax
+from jax.experimental import pallas as pl
+from jax.experimental.pallas import tpu as pltpu
 from jax.sharding import PartitionSpec as P
 
 EXPERTS = 32
@@ -98,12 +100,266 @@
     return jnp.einsum("rke,rkc,rk->rec", expert_hot, place_hot, route_weight)
 
 
-def expert_hidden(piece, gate_weight, up_weight):
-    gate_pre = jnp.einsum("aecd,edf->aecf", piece, gate_weight, preferred_element_type=jnp.float32)
-    up_pre = jnp.einsum("aecd,edf->aecf", piece, up_weight, preferred_element_type=jnp.float32)
-    clipped = jnp.minimum(gate_pre, CLAMP_LIMIT)
-    linear = jnp.clip(up_pre, -CLAMP_LIMIT, CLAMP_LIMIT)
-    return (clipped * jax.nn.sigmoid(ACT_SLOPE * clipped) * (linear + 1.0)).astype(jnp.bfloat16)
+CHAINS = ((0, 1, 4), (0, -1, 3), (1, 1, 3), (1, -1, 4))
+HOPS = {}
+for _half, _way, _far in CHAINS:
+    for _hop in range(1, _far + 1):
+        HOPS[_half, _way, _hop] = len(HOPS)
+VMEM_LIMIT = 60 * 1024 * 1024
+
+
+def remote(source, target, send_sem, recv_sem, where):
+    return pltpu.make_async_remote_copy(
+        src_ref=source,
+        dst_ref=target,
+        send_sem=send_sem,
+        recv_sem=recv_sem,
+        device_id=where,
+        device_id_type=pl.DeviceIdType.MESH,
+    )
+
+
+def greet(places):
+    barrier = pltpu.get_barrier_semaphore()
+    for place in places:
+        pl.semaphore_signal(
+            barrier, inc=1, device_id=place, device_id_type=pl.DeviceIdType.MESH
+        )
+    pl.semaphore_wait(barrier, len(places))
+
+
+def exchange_kernel(axis, count, x_ref, out_ref, send_sem, recv_sem):
+    me = lax.axis_index(axis)
+    barrier = pltpu.get_barrier_semaphore()
+
+    def hello(step, carry):
+        place = {axis: lax.rem(me + step, count)}
+        pl.semaphore_signal(
+            barrier, inc=1, device_id=place, device_id_type=pl.DeviceIdType.MESH
+        )
+        return carry
+
+    lax.fori_loop(1, count, hello, 0)
+    pl.semaphore_wait(barrier, count - 1)
+
+    def copy_for(step):
+        peer = lax.rem(me + step, count)
+        return remote(
+            x_ref.at[peer], out_ref.at[me], send_sem.at[step], recv_sem.at[step], {axis: peer}
+        )
+
+    def begin(step, carry):
+        copy_for(step).start()
+        return carry
+
+    def end(step, carry):
+        copy_for(step).wait()
+        return carry
+
+    lax.fori_loop(1, count, begin, 0)
+    out_ref[me] = x_ref[me]
+    lax.fori_loop(1, count, end, 0)
+
+
+def exchange(value, axis, collective_id):
+    count = value.shape[0]
+    return pl.pallas_call(
+        lambda *refs: exchange_kernel(axis, count, *refs),
+        out_shape=jax.ShapeDtypeStruct(value.shape, value.dtype),
+        in_specs=[pl.BlockSpec(memory_space=pltpu.VMEM)],
+        out_specs=pl.BlockSpec(memory_space=pltpu.VMEM),
+        scratch_shapes=[
+            pltpu.SemaphoreType.DMA((count,)),
+            pltpu.SemaphoreType.DMA((count,)),
+        ],
+        compiler_params=pltpu.CompilerParams(
+            collective_id=collective_id, has_side_effects=True
+        ),
+        cost_estimate=pl.CostEstimate(
+            flops=100000000, bytes_accessed=2 * value.size * 2, transcendentals=0
+        ),
+        name="exchange_" + axis,
+    )(value)
+
+
+def ring_kernel(
+    x_ref,
+    gate_ref,
+    up_ref,
+    down_ref,
+    out_ref,
+    w1,
+    w2,
+    xbuf,
+    pbuf,
+    rbuf,
+    wl_sem,
+    ws_sem,
+    wr_sem,
+    gs_sem,
+    gr_sem,
+    ss_sem,
+    sr_sem,
+):
+    tp = lax.axis_index("tp")
+    ring = lax.axis_size("tp") // 2
+    core = lax.rem(tp, 2)
+    spot = lax.div(tp, 2)
+    ahead = {"tp": lax.rem(spot + 1, ring) * 2 + core}
+    behind = {"tp": lax.rem(spot + ring - 1, ring) * 2 + core}
+    partner = {"tp": spot * 2 + (1 - core)}
+    rows = x_ref.shape[0]
+    part = rows // 2
+    inner = down_ref.shape[1]
+    local = [
+        pltpu.make_async_copy(gate_ref.at[0], w1.at[:, pl.ds(0, inner)], wl_sem.at[0]),
+        pltpu.make_async_copy(up_ref.at[0], w1.at[:, pl.ds(2 * inner, inner)], wl_sem.at[1]),
+        pltpu.make_async_copy(down_ref.at[0], w2.at[pl.ds(0, inner)], wl_sem.at[2]),
+    ]
+    for copy in local:
+        copy.start()
+    greet((ahead, behind, partner))
+
+    def half_rows(half):
+        return pl.ds(half * part, part)
+
+    def gather_copy(half, way, hop):
+        slot = (-way * (hop - 1)) % ring
+        source = x_ref.at[half_rows(half)] if hop == 1 else xbuf.at[slot, half_rows(half)]
+        number = HOPS[half, way, hop]
+        return remote(
+            source,
+            xbuf.at[(-way * hop) % ring, half_rows(half)],
+            gs_sem.at[number],
+            gr_sem.at[number],
+            ahead if way == 1 else behind,
+        )
+
+    def sum_copy(half, way, hop):
+        number = HOPS[half, way, hop]
+        return remote(
+            pbuf.at[(way * hop) % ring, half_rows(half)],
+            rbuf.at[number],
+            ss_sem.at[number],
+            sr_sem.at[number],
+            ahead if way == 1 else behind,
+        )
+
+    for half, way in ((0, 1), (1, -1), (1, 1), (0, -1)):
+        gather_copy(half, way, 1).start()
+    shared = [
+        remote(
+            gate_ref.at[0], w1.at[:, pl.ds(inner, inner)], ws_sem.at[0], wr_sem.at[0], partner
+        ),
+        remote(
+            up_ref.at[0], w1.at[:, pl.ds(3 * inner, inner)], ws_sem.at[1], wr_sem.at[1], partner
+        ),
+        remote(down_ref.at[0], w2.at[pl.ds(inner, inner)], ws_sem.at[2], wr_sem.at[2], partner),
+    ]
+    for copy in shared:
+        copy.start()
+    for copy in local:
+        copy.wait()
+    for copy in shared:
+        copy.wait_recv()
+
+    def experts(rows_in, slot):
+        pre = jnp.dot(rows_in, w1[...], preferred_element_type=jnp.float32)
+        clipped = jnp.minimum(pre[:, : 2 * inner], CLAMP_LIMIT)
+        linear = jnp.clip(pre[:, 2 * inner :], -CLAMP_LIMIT, CLAMP_LIMIT)
+        hidden = (clipped * jax.nn.sigmoid(ACT_SLOPE * clipped) * (linear + 1.0)).astype(
+            jnp.bfloat16
+        )
+        width = w2.shape[1]
+        step = width // 4
+        for at in range(0, width, step):
+            pbuf[slot, :, at : at + step] = jnp.dot(
+                hidden, w2[:, at : at + step], preferred_element_type=jnp.float32
+            ).astype(jnp.bfloat16)
+
+    experts(x_ref[...], 0)
+    for hop in range(1, 5):
+        for half, way, far in ((0, 1, 4), (1, -1, 4), (1, 1, 3), (0, -1, 3)):
+            if hop <= far:
+                gather_copy(half, way, hop).wait_recv()
+                if hop < far:
+                    gather_copy(half, way, hop + 1).start()
+        if hop < 4:
+
+            def both(index, carry, hop=hop):
+                slot = hop + index * (ring - 2 * hop)
+                experts(xbuf[slot], slot)
+                return carry
+
+            lax.fori_loop(0, 2, both, 0)
+        else:
+            experts(xbuf[4], 4)
+        if hop >= 3:
+            for half, way, far in ((0, 1, 4), (1, -1, 4), (1, 1, 3), (0, -1, 3)):
+                if far == hop:
+                    sum_copy(half, way, far).start()
+    for left in (3, 2, 1, 0):
+        for half, way, far in ((1, 1, 3), (0, -1, 3), (0, 1, 4), (1, -1, 4)):
+            hop = far - (4 - left) + 1
+            if hop < 1:
+                continue
+            sum_copy(half, way, hop).wait_recv()
+            if hop > 1:
+                slot = (way * (hop - 1)) % ring
+                at = half_rows(half)
+                pbuf[slot, at] = (
+                    pbuf[slot, at].astype(jnp.float32)
+                    + rbuf[HOPS[half, way, hop]].astype(jnp.float32)
+                ).astype(jnp.bfloat16)
+                sum_copy(half, way, hop - 1).start()
+    for half in range(2):
+        at = half_rows(half)
+        out_ref[at] = (
+            pbuf[0, at].astype(jnp.float32)
+            + rbuf[HOPS[half, 1, 1]].astype(jnp.float32)
+            + rbuf[HOPS[half, -1, 1]].astype(jnp.float32)
+        ).astype(jnp.bfloat16)
+    for copy in shared:
+        copy.wait_send()
+    for half, way, hop in HOPS:
+        gather_copy(half, way, hop).wait_send()
+        sum_copy(half, way, hop).wait_send()
+
+
+def ring_experts(x, gate_weight, up_weight, down_weight):
+    rows, width = x.shape
+    inner = down_weight.shape[1]
+    ring = lax.axis_size("tp") // 2
+    copies = len(HOPS)
+    dma = pltpu.SemaphoreType.DMA
+    return pl.pallas_call(
+        ring_kernel,
+        out_shape=jax.ShapeDtypeStruct(x.shape, x.dtype),
+        in_specs=[pl.BlockSpec(memory_space=pltpu.VMEM)]
+        + [pl.BlockSpec(memory_space=pl.ANY)] * 3,
+        out_specs=pl.BlockSpec(memory_space=pltpu.VMEM),
+        scratch_shapes=[
+            pltpu.VMEM((width, 4 * inner), jnp.bfloat16),
+            pltpu.VMEM((2 * inner, width), jnp.bfloat16),
+            pltpu.VMEM((ring, rows, width), jnp.bfloat16),
+            pltpu.VMEM((ring, rows, width), jnp.bfloat16),
+            pltpu.VMEM((copies, rows // 2, width), jnp.bfloat16),
+            dma((3,)),
+            dma((3,)),
+            dma((3,)),
+            dma((copies,)),
+            dma((copies,)),
+            dma((copies,)),
+            dma((copies,)),
+        ],
+        compiler_params=pltpu.CompilerParams(
+            collective_id=3, has_side_effects=True, vmem_limit_bytes=VMEM_LIMIT
+        ),
+        cost_estimate=pl.CostEstimate(
+            flops=2500000000, bytes_accessed=8000000, transcendentals=200000
+        ),
+        name="ring_experts",
+    )(x, gate_weight, up_weight, down_weight)
 
 
 def on_device(
@@ -133,8 +389,6 @@
     fanout = routes.shape[1]
     capacity = (3 * own_rows * fanout + 2 * EXPERTS - 1) // (2 * EXPERTS)
     ep_size = lax.axis_size("ep")
-    tp_size = lax.axis_size("tp")
-    local_experts = gate_weight.shape[0]
     widened = expert_input.astype(jnp.float32)
     normed = (
         widened
@@ -147,19 +401,12 @@
     slot_rows = jnp.einsum(
         "ecr,rd->ecd", sender, normed, preferred_element_type=jnp.float32
     ).astype(jnp.bfloat16)
-    slot_rows = slot_rows.reshape(ep_size, local_experts, capacity, -1)
-    arrived = lax.all_to_all(slot_rows, "ep", split_axis=0, concat_axis=0, tiled=True)
-    hidden_units = expert_hidden(
-        lax.all_gather(arrived, "tp", axis=0, tiled=True), gate_weight, up_weight
-    )
-    partial_value = jnp.einsum(
-        "aecf,efd->aecd", hidden_units, down_weight, preferred_element_type=jnp.float32
-    ).astype(jnp.bfloat16)
-    partial_value = partial_value.reshape(tp_size, ep_size * local_experts * capacity, -1)
-    pieces = lax.all_to_all(partial_value, "tp", split_axis=0, concat_axis=0, tiled=True)
-    summed = jnp.sum(pieces, axis=0, dtype=jnp.float32).astype(jnp.bfloat16)
-    summed = summed.reshape(ep_size, local_experts * capacity, -1)
-    returned = lax.all_to_all(summed, "ep", split_axis=0, concat_axis=0, tiled=True)
+    messages = slot_rows.reshape(ep_size, -1, 128)
+    arrived = exchange(messages, "ep", 1)
+    width = expert_input.shape[1]
+    summed = ring_experts(arrived.reshape(-1, width), gate_weight, up_weight, down_weight)
+    returned = exchange(summed.reshape(messages.shape), "ep", 2)
+    returned = returned.reshape(EXPERTS, capacity, width)
     expert_mix = jnp.einsum("rec,ecd->rd", combine, returned.astype(jnp.float32)).astype(
         jnp.bfloat16
     )

time: 329 us -> 158 us (0.48)
  the two profiles are of different devices: /device:TPU:24 before, /device:TPU:16 now
where the time goes in v1:
time: 158 us; the launch traced here: 157 us
  Pallas kernels  120 us (76%)
  between operations  14.4 us (9%)
  local copies, waits for them, and re-layouts  9.08 us (6%)
  matrix products  5.09 us (3%)
  other arithmetic  5.06 us (3%)
  starting transfers between devices  3.43 us (2%)
    pallas_call x1, Pallas kernels, ring_experts(): pl.pallas_call(ring_kernel, out_shape=jax.ShapeDtypeStruct(x.shape, x.dty...  74.6 us
    pallas_call x2, Pallas kernels, exchange(): pl.pallas_call(lambda *refs: exchange_kernel(axis, count, *refs), out_sha...  45.4 us
    ppermute x1, starting transfers between devices, shifted(): lax.ppermute(value, axis, [(source, source + steps) for source in range(i...  3.4 us
  transfers between devices with their start and end apart: 2, of which 0 were waited for; matrix products, arithmetic and copies ran while one was open for 8% of the time, Pallas kernels for 76%

profile of v1, /device:TPU:16, one launch (start us, length us, event | category | flops | bytes accessed | tf_op | source)
XLA Modules:
  0.0 157.0 jit_solution(9646688570608177240)
XLA Ops:
  7.3 1.0 fusion.19
  8.3 0.9 fusion.21
  9.2 0.7 slice_bitcast_fusion.2
  9.9 3.4 %collective-permute-start = (bf16[2,128,1,64]{1,3,2,0:T(8,128)(2,1)S(1)}, bf16[2,128,1,64]{1,3,2,0:T(8,128)(2,1)S(1)}, u32[]{:S(2)}, u32[]{:S(2)}) collective-permute-start(bf16[2,128,1,64]{1,3,2,0:T(8,128)(2,1)S(1)} %pad_maximum_fusion.2), channel_id=1, source_target_pairs={{0,16},{16,32},{32,48},{48,64},{64,80},{80,96},{96,112},{112,128},... | collective-permute-start | bytes 98312 | tf_op jit(solution)/shard_map/ppermute | solution.py:21
  13.3 0.9 fusion.58
  14.3 1.0 convert_multiply_fusion.4
  15.9 0.5 fusion.56
  16.5 0.2 fusion.1
  16.8 0.4 fusion.4
  17.3 2.1 %convolution_convert_fusion = bf16[512,2048]{1,0:T(8,128)(2,1)} fusion(bf16[192,2048]{1,0:T(8,128)(2,1)S(1)} %copy-done, bf16[24,8,4,128]{3,2,1,0:T(4,128)(2,1)S(1)} %bitcast.75), kind=kOutput, calls=%fused_computation | convolution fusion | flops 403701760 | bytes 3080192 | tf_op jit(solution)/shard_map/dot_general | solution.py:383
  19.5 0.6 copy-done.7
  20.5 0.2 select_reduce_fusion
  21.0 0.4 fusion.39
  21.6 0.3 convolution_convert_fusion.1
  21.9 0.3 copy.34
  22.3 1.2 reshape.194.refs_0_
  23.5 25.4 %exchange_ep.2 = bf16[32,48,128]{2,1,0:T(8,128)(2,1)} custom-call(bf16[32,48,128]{2,1,0:T(8,128)(2,1)} %reshape.194.refs_0_), custom_call_target="tpu_custom_call" | custom-call | flops 100000000 | bytes 786432 | tf_op jit(solution)/shard_map/exchange_ep/pallas_call | solution.py:166
  48.8 1.9 %reshape.195.x_ref = bf16[96,2048]{1,0:T(8,128)(2,1)} reshape(bf16[32,48,128]{2,1,0:T(8,128)(2,1)} %exchange_ep.2) | data formatting | bytes 786432 | tf_op jit(solution)/shard_map/reshape | solution.py:407
  50.7 74.6 %ring_experts.1 = bf16[96,2048]{1,0:T(8,128)(2,1)} custom-call(bf16[96,2048]{1,0:T(8,128)(2,1)} %reshape.195.x_ref, bf16[1,2048,128]{2,1,0:T(8,128)(2,1)} %gate_ref.1, bf16[1,2048,128]{2,1,0:T(8,128)(2,1)} %up_ref.1, bf16[1,128,2048]{2,1,0:T(8,128)(2,1)} %down_ref.1), custom_call_target="tpu_custom_call" | custom-call | flops 2500000000 | bytes 8000000 | tf_op jit(solution)/shard_map/ring_experts/pallas_call | solution.py:335
  125.3 1.9 %reshape.196.refs_0_ = bf16[32,48,128]{2,1,0:T(8,128)(2,1)} reshape(bf16[96,2048]{1,0:T(8,128)(2,1)} %ring_experts.1) | data formatting | bytes 786432 | tf_op jit(solution)/shard_map/reshape | solution.py:408
  127.3 20.1 %exchange_ep.3 = bf16[32,48,128]{2,1,0:T(8,128)(2,1)} custom-call(bf16[32,48,128]{2,1,0:T(8,128)(2,1)} %reshape.196.refs_0_), custom_call_target="tpu_custom_call" | custom-call | flops 100000000 | bytes 786432 | tf_op jit(solution)/shard_map/exchange_ep/pallas_call | solution.py:166
  147.3 1.4 reshape.197
  148.7 0.4 fusion.37
  149.1 1.1 fusion
  (53 shorter events, 1.8 us)
Async XLA Ops:
  7.2 10.2 %copy-start = (bf16[192,2048]{1,0:T(8,128)(2,1)S(1)}, bf16[192,2048]{1,0:T(8,128)(2,1)}, u32[]{:S(2)}) copy-start(bf16[192,2048]{1,0:T(8,128)(2,1)} %param.20) | copy-start | bytes 2359300
  7.2 8.5 %copy-start.3 = (bf16[512,64]{0,1:T(8,128)(2,1)S(1)}, bf16[512,64]{0,1:T(8,128)(2,1)}, u32[]{:S(2)}) copy-start(bf16[512,64]{0,1:T(8,128)(2,1)} %param.16) | copy-start | bytes 196612
  7.2 8.4 %copy-start.1 = (bf16[512,192]{0,1:T(8,128)(2,1)S(1)}, bf16[512,192]{0,1:T(8,128)(2,1)}, u32[]{:S(2)}) copy-start(bf16[512,192]{0,1:T(8,128)(2,1)} %param.14) | copy-start | bytes 589828
  7.2 8.7 %copy-start.8 = (f32[3,64]{1,0:T(4,128)S(1)}, f32[3,64]{1,0:T(4,128)}, u32[]{:S(2)}) copy-start(f32[3,64]{1,0:T(4,128)} %param.17) | copy-start | bytes 2308
  7.2 143.0 %reduce-scatter.2.cloned.1.call-start = ((), (), s32[]{:S(2)}) async-start(), calls=%async_computation.1 | async-start | bytes 2228224 | tf_op jit(solution)/shard_map/reduce_scatter | solution.py:382
  9.9 5.9 %collective-permute-start = (bf16[2,128,1,64]{1,3,2,0:T(8,128)(2,1)S(1)}, bf16[2,128,1,64]{1,3,2,0:T(8,128)(2,1)S(1)}, u32[]{:S(2)}, u32[]{:S(2)}) collective-permute-start(bf16[2,128,1,64]{1,3,2,0:T(8,128)(2,1)S(1)} %pad_maximum_fusion.2), channel_id=1, source_target_pairs={{0,16},{16,32},{32,48},{48,64},{64,80},{80,96},{96,112},{112,128},... | collective-permute-start | bytes 98312 | tf_op jit(solution)/shard_map/ppermute | solution.py:21
  15.7 0.7 copy-start.6
  19.4 0.7 copy-start.7
  19.4 1.3 copy-start.4
  19.5 2.0 %copy-start.2 = (bf16[32,2048]{1,0:T(8,128)(2,1)S(1)}, bf16[32,2048]{1,0:T(8,128)(2,1)}, u32[]{:S(2)}) copy-start(bf16[32,2048]{1,0:T(8,128)(2,1)} %param.21) | copy-start | bytes 393220
  19.5 2.1 %copy-start.5 = (f32[2048]{0:T(1024)S(1)}, f32[2048]{0:T(1024)}, u32[]{:S(2)}) copy-start(f32[2048]{0:T(1024)} %param.22) | copy-start | bytes 24580
Sparse Core Ops, SparseCore 0:
  19.6 66.5 reduce-scatter.1

commit v2 on v1

--- a/solution.py
+++ b/solution.py
@@ -105,6 +105,7 @@
 for _half, _way, _far in CHAINS:
     for _hop in range(1, _far + 1):
         HOPS[_half, _way, _hop] = len(HOPS)
+X_RING = 4
 VMEM_LIMIT = 60 * 1024 * 1024
 
 
@@ -128,43 +129,64 @@
     pl.semaphore_wait(barrier, len(places))
 
 
-def exchange_kernel(axis, count, x_ref, out_ref, send_sem, recv_sem):
-    me = lax.axis_index(axis)
-    barrier = pltpu.get_barrier_semaphore()
-
-    def hello(step, carry):
-        place = {axis: lax.rem(me + step, count)}
-        pl.semaphore_signal(
-            barrier, inc=1, device_id=place, device_id_type=pl.DeviceIdType.MESH
+def neighbours():
+    tp = lax.axis_index("tp")
+    ring = lax.axis_size("tp") // 2
+    core, spot = lax.rem(tp, 2), lax.div(tp, 2)
+    ahead = {"tp": lax.rem(spot + 1, ring) * 2 + core}
+    behind = {"tp": lax.rem(spot + ring - 1, ring) * 2 + core}
+    partner = {"tp": spot * 2 + (1 - core)}
+    return ring, core, spot, ahead, behind, partner
+
+
+def exchange_order(count):
+    long = count // X_RING
+    turns = [1, long - 1, 2, long - 2, 3, long - 3, long // 2, 0]
+    return [
+        (along, across) for across in (0, 1, X_RING - 1, 2) for along in turns if along or across
+    ]
+
+
+def ep_place(me, offset):
+    along, across = offset
+    z, x = lax.div(me, X_RING), lax.rem(me, X_RING)
+    return (
+        lax.rem(z + along, lax.axis_size("ep") // X_RING) * X_RING + lax.rem(x + across, X_RING)
+    )
+
+
+def exchange_copies(x_ref, out_ref, send_sem, recv_sem):
+    me = lax.axis_index("ep")
+    copies = []
+    for number, offset in enumerate(exchange_order(lax.axis_size("ep"))):
+        peer = ep_place(me, offset)
+        copies.append(
+            remote(
+                x_ref.at[peer],
+                out_ref.at[me],
+                send_sem.at[number],
+                recv_sem.at[number],
+                {"ep": peer},
+            )
         )
-        return carry
-
-    lax.fori_loop(1, count, hello, 0)
-    pl.semaphore_wait(barrier, count - 1)
-
-    def copy_for(step):
-        peer = lax.rem(me + step, count)
-        return remote(
-            x_ref.at[peer], out_ref.at[me], send_sem.at[step], recv_sem.at[step], {axis: peer}
-        )
-
-    def begin(step, carry):
-        copy_for(step).start()
-        return carry
-
-    def end(step, carry):
-        copy_for(step).wait()
-        return carry
-
-    lax.fori_loop(1, count, begin, 0)
+    return copies
+
+
+def exchange_kernel(x_ref, out_ref, send_sem, recv_sem):
+    me = lax.axis_index("ep")
+    greet([{"ep": ep_place(me, offset)} for offset in exchange_order(lax.axis_size("ep"))])
+    copies = exchange_copies(x_ref, out_ref, send_sem, recv_sem)
+    for copy in copies:
+        copy.start()
     out_ref[me] = x_ref[me]
-    lax.fori_loop(1, count, end, 0)
-
-
-def exchange(value, axis, collective_id):
+    for copy in copies:
+        copy.wait()
+
+
+def exchange(value, collective_id):
     count = value.shape[0]
     return pl.pallas_call(
-        lambda *refs: exchange_kernel(axis, count, *refs),
+        exchange_kernel,
         out_shape=jax.ShapeDtypeStruct(value.shape, value.dtype),
         in_specs=[pl.BlockSpec(memory_space=pltpu.VMEM)],
         out_specs=pl.BlockSpec(memory_space=pltpu.VMEM),
@@ -175,11 +197,121 @@
         compiler_params=pltpu.CompilerParams(
             collective_id=collective_id, has_side_effects=True
         ),
-        cost_estimate=pl.CostEstimate(
-            flops=100000000, bytes_accessed=2 * value.size * 2, transcendentals=0
-        ),
-        name="exchange_" + axis,
+        name="exchange_ep",
     )(value)
+
+
+def finish_kernel(
+    x_ref,
+    part_ref,
+    out_ref,
+    attended_ref,
+    swapped,
+    pair,
+    rbuf,
+    send_sem,
+    recv_sem,
+    swap_sem,
+    ss_sem,
+    sr_sem,
+):
+    me = lax.axis_index("ep")
+    ring, core, spot, ahead, behind, partner = neighbours()
+    rows = attended_ref.shape[0]
+    part = rows // 2
+    greet(
+        [ahead, behind, partner]
+        + [{"ep": ep_place(me, offset)} for offset in exchange_order(lax.axis_size("ep"))]
+    )
+    swap = remote(part_ref.at[:, 1 - core], swapped, swap_sem.at[0], swap_sem.at[1], partner)
+    swap.start()
+    copies = exchange_copies(x_ref, out_ref, send_sem, recv_sem)
+    for copy in copies:
+        copy.start()
+    out_ref[me] = x_ref[me]
+
+    def half_rows(half):
+        return pl.ds(half * part, part)
+
+    def sum_copy(half, way, hop):
+        number = HOPS[half, way, hop]
+        return remote(
+            pair.at[(way * hop) % ring, half_rows(half)],
+            rbuf.at[number],
+            ss_sem.at[number],
+            sr_sem.at[number],
+            ahead if way == 1 else behind,
+        )
+
+    swap.wait_recv()
+    for slot in (4, 3, 5, 2, 6, 1, 7, 0):
+        owner = lax.rem(spot + slot, ring)
+        pair[slot] = (
+            part_ref[owner, core].astype(jnp.float32) + swapped[owner].astype(jnp.float32)
+        ).astype(jnp.bfloat16)
+        if slot == 4:
+            sum_copy(0, 1, 4).start()
+            sum_copy(1, -1, 4).start()
+        if slot == 3:
+            sum_copy(1, 1, 3).start()
+        if slot == 5:
+            sum_copy(0, -1, 3).start()
+    for left in (3, 2, 1, 0):
+        for half, way, far in ((0, 1, 4), (1, -1, 4), (1, 1, 3), (0, -1, 3)):
+            hop = far - (4 - left) + 1
+            if hop < 1:
+                continue
+            sum_copy(half, way, hop).wait_recv()
+            if hop > 1:
+                slot = (way * (hop - 1)) % ring
+                at = half_rows(half)
+                pair[slot, at] = (
+                    pair[slot, at].astype(jnp.float32)
+                    + rbuf[HOPS[half, way, hop]].astype(jnp.float32)
+                ).astype(jnp.bfloat16)
+                sum_copy(half, way, hop - 1).start()
+    for half in range(2):
+        at = half_rows(half)
+        attended_ref[at] = (
+            pair[0, at].astype(jnp.float32)
+            + rbuf[HOPS[half, 1, 1]].astype(jnp.float32)
+            + rbuf[HOPS[half, -1, 1]].astype(jnp.float32)
+        ).astype(jnp.bfloat16)
+    swap.wait_send()
+    for half, way, hop in HOPS:
+        sum_copy(half, way, hop).wait_send()
+    for copy in copies:
+        copy.wait()
+
+
+def finish(value, partial_rows):
+    count = value.shape[0]
+    ring = lax.axis_size("tp") // 2
+    rows, width = partial_rows.shape[0] // (2 * ring), partial_rows.shape[1]
+    dma = pltpu.SemaphoreType.DMA
+    return pl.pallas_call(
+        finish_kernel,
+        out_shape=(
+            jax.ShapeDtypeStruct(value.shape, value.dtype),
+            jax.ShapeDtypeStruct((rows, width), jnp.bfloat16),
+        ),
+        in_specs=[pl.BlockSpec(memory_space=pltpu.VMEM)] * 2,
+        out_specs=[pl.BlockSpec(memory_space=pltpu.VMEM)] * 2,
+        scratch_shapes=[
+            pltpu.VMEM((ring, rows, width), jnp.bfloat16),
+            pltpu.VMEM((ring, rows, width), jnp.bfloat16),
+            pltpu.VMEM((len(HOPS), rows // 2, width), jnp.bfloat16),
+            dma((count,)),
+            dma((count,)),
+            dma((2,)),
+            dma((len(HOPS),)),
+            dma((len(HOPS),)),
+        ],
+        compiler_params=pltpu.CompilerParams(
+            collective_id=2, has_side_effects=True, vmem_limit_bytes=VMEM_LIMIT
+        ),
+        name="finish",
+    )(value, partial_rows.reshape(ring, 2, rows, width))
 
 
 def ring_kernel(
@@ -201,13 +333,7 @@
     ss_sem,
     sr_sem,
 ):
-    tp = lax.axis_index("tp")
-    ring = lax.axis_size("tp") // 2
-    core = lax.rem(tp, 2)
-    spot = lax.div(tp, 2)
-    ahead = {"tp": lax.rem(spot + 1, ring) * 2 + core}
-    behind = {"tp": lax.rem(spot + ring - 1, ring) * 2 + core}
-    partner = {"tp": spot * 2 + (1 - core)}
+    ring, core, spot, ahead, behind, partner = neighbours()
     rows = x_ref.shape[0]
     part = rows // 2
     inner = down_ref.shape[1]
@@ -379,11 +505,8 @@
     down_weight,
 ):
     heads_out = attend(query_rows, key_rows, value_rows, query_gain, key_gain, sink_logits)
-    attended = lax.psum_scatter(
-        jnp.dot(heads_out, out_weight, preferred_element_type=jnp.float32).astype(jnp.bfloat16),
-        "tp",
-        scatter_dimension=0,
-        tiled=True,
+    partial_rows = jnp.dot(heads_out, out_weight, preferred_element_type=jnp.float32).astype(
+        jnp.bfloat16
     )
     own_rows = expert_input.shape[0]
     fanout = routes.shape[1]
@@ -402,10 +525,10 @@
         "ecr,rd->ecd", sender, normed, preferred_element_type=jnp.float32
     ).astype(jnp.bfloat16)
     messages = slot_rows.reshape(ep_size, -1, 128)
-    arrived = exchange(messages, "ep", 1)
+    arrived = exchange(messages, 1)
     width = expert_input.shape[1]
     summed = ring_experts(arrived.reshape(-1, width), gate_weight, up_weight, down_weight)
-    returned = exchange(summed.reshape(messages.shape), "ep", 2)
+    returned, attended = finish(summed.reshape(messages.shape), partial_rows)
     returned = returned.reshape(EXPERTS, capacity, width)
     expert_mix = jnp.einsum("rec,ecd->rd", combine, returned.astype(jnp.float32)).astype(
         jnp.bfloat16

time: 158 us -> 149 us (0.943)
  the two profiles are of different devices: /device:TPU:16 before, /device:TPU:9 now
where the time goes in v2:
time: 149 us; the launch traced here: 148 us
  Pallas kernels  121 us (81%)
  local copies, waits for them, and re-layouts  10.7 us (7%)
  other arithmetic  7.02 us (5%)
  matrix products  5.08 us (3%)
  starting transfers between devices  3.12 us (2%)
    pallas_call x1, Pallas kernels, ring_experts(): pl.pallas_call(ring_kernel, out_shape=jax.ShapeDtypeStruct(x.shape, x.dty...  66.4 us
    pallas_call x1, Pallas kernels, finish(): pl.pallas_call(finish_kernel, out_shape=(jax.ShapeDtypeStruct(value.shape...  29.4 us
    pallas_call x1, Pallas kernels, exchange(): pl.pallas_call(exchange_kernel, out_shape=jax.ShapeDtypeStruct(value.shap...  25.5 us
    ppermute x1, starting transfers between devices, shifted(): lax.ppermute(value, axis, [(source, source + steps) for source in range(i...  3.12 us
  transfers between devices with their start and end apart: 1, of which 0 were waited for; matrix products, arithmetic and copies ran while one was open for 8% of the time, Pallas kernels for 62%

profile of v2, /device:TPU:9, one launch (start us, length us, event | category | flops | bytes accessed | tf_op | source)
XLA Modules:
  0.0 148.1 jit_solution(9443596573522095084)
XLA Ops:
  0.7 0.9 fusion.19
  1.6 0.9 fusion.21
  2.6 0.7 slice_bitcast_fusion.2
  3.3 3.1 %collective-permute-start = (bf16[2,128,1,64]{1,3,2,0:T(8,128)(2,1)S(1)}, bf16[2,128,1,64]{1,3,2,0:T(8,128)(2,1)S(1)}, u32[]{:S(2)}, u32[]{:S(2)}) collective-permute-start(bf16[2,128,1,64]{1,3,2,0:T(8,128)(2,1)S(1)} %pad_maximum_fusion.2), channel_id=1, source_target_pairs={{0,16},{16,32},{32,48},{48,64},{64,80},{80,96},{96,112},{112,128},... | collective-permute-start | bytes 98312 | tf_op jit(solution)/shard_map/ppermute | solution.py:21
  6.4 0.9 fusion.58
  7.4 0.7 reduce_max.19
  8.1 0.7 fusion.52
  8.8 0.7 fusion.51
  9.5 1.0 fusion.11
  10.6 0.8 copy.23
  12.0 0.4 fusion.40
  12.4 0.4 fusion.37
  13.6 1.2 reshape.191.x_ref
  14.8 25.5 %exchange_ep.1 = bf16[32,48,128]{2,1,0:T(8,128)(2,1)} custom-call(bf16[32,48,128]{2,1,0:T(8,128)(2,1)} %reshape.191.x_ref), custom_call_target="tpu_custom_call" | custom-call | tf_op jit(solution)/shard_map/exchange_ep/pallas_call | solution.py:188
  40.3 1.9 %reshape.192.x_ref = bf16[96,2048]{1,0:T(8,128)(2,1)} reshape(bf16[32,48,128]{2,1,0:T(8,128)(2,1)} %exchange_ep.1) | data formatting | bytes 786432 | tf_op jit(solution)/shard_map/reshape | solution.py:530
  42.4 66.4 %ring_experts.1 = bf16[96,2048]{1,0:T(8,128)(2,1)} custom-call(bf16[96,2048]{1,0:T(8,128)(2,1)} %reshape.192.x_ref, bf16[1,2048,128]{2,1,0:T(8,128)(2,1)} %gate_ref.1, bf16[1,2048,128]{2,1,0:T(8,128)(2,1)} %up_ref.1, bf16[1,128,2048]{2,1,0:T(8,128)(2,1)} %down_ref.1), custom_call_target="tpu_custom_call" | custom-call | flops 2500000000 | bytes 8000000 | tf_op jit(solution)/shard_map/ring_experts/pallas_call | solution.py:461
  109.1 1.9 %reshape.193.x_ref = bf16[32,48,128]{2,1,0:T(8,128)(2,1)} reshape(bf16[96,2048]{1,0:T(8,128)(2,1)} %ring_experts.1) | data formatting | bytes 786432 | tf_op jit(solution)/shard_map/reshape | solution.py:531
  111.1 0.5 fusion.56
  112.0 0.4 fusion.4
  112.5 2.1 %convolution_convert_fusion = bf16[512,2048]{1,0:T(8,128)(2,1)} fusion(bf16[192,2048]{1,0:T(8,128)(2,1)S(1)} %copy-done, bf16[24,8,4,128]{3,2,1,0:T(4,128)(2,1)S(1)} %bitcast.77), kind=kOutput, calls=%fused_computation | convolution fusion | flops 403701760 | bytes 3080192 | tf_op jit(solution)/shard_map/dot_general | solution.py:508
  114.6 29.4 %finish.1 = (bf16[32,48,128]{2,1,0:T(8,128)(2,1)}, bf16[32,2048]{1,0:T(8,128)(2,1)}) custom-call(bf16[32,48,128]{2,1,0:T(8,128)(2,1)} %reshape.193.x_ref, bf16[8,2,32,2048]{3,2,1,0:T(8,128)(2,1)} %bitcast.75), custom_call_target="tpu_custom_call" | custom-call | tf_op jit(solution)/shard_map/finish/pallas_call | solution.py:292
  144.0 1.4 reshape.201
  145.4 1.1 fusion
  146.5 1.6 %copy.63 = bf16[32,2048]{1,0:T(8,128)(2,1)} copy(bf16[32,2048]{1,0:T(8,128)(2,1)} %get-tuple-element.14) | data formatting | bytes 262144
  (47 shorter events, 2.5 us)
Async XLA Ops:
  0.6 111.9 %copy-start = (bf16[192,2048]{1,0:T(8,128)(2,1)S(1)}, bf16[192,2048]{1,0:T(8,128)(2,1)}, u32[]{:S(2)}) copy-start(bf16[192,2048]{1,0:T(8,128)(2,1)} %param.20) | copy-start | bytes 2359300
  0.6 12.2 %copy-start.2 = (bf16[32,2048]{1,0:T(8,128)(2,1)S(1)}, bf16[32,2048]{1,0:T(8,128)(2,1)}, u32[]{:S(2)}) copy-start(bf16[32,2048]{1,0:T(8,128)(2,1)} %param.21) | copy-start | bytes 393220
  0.7 12.2 %copy-start.4 = (f32[2048]{0:T(1024)S(1)}, f32[2048]{0:T(1024)}, u32[]{:S(2)}) copy-start(f32[2048]{0:T(1024)} %param.22) | copy-start | bytes 24580
  3.3 107.8 %collective-permute-start = (bf16[2,128,1,64]{1,3,2,0:T(8,128)(2,1)S(1)}, bf16[2,128,1,64]{1,3,2,0:T(8,128)(2,1)S(1)}, u32[]{:S(2)}, u32[]{:S(2)}) collective-permute-start(bf16[2,128,1,64]{1,3,2,0:T(8,128)(2,1)S(1)} %pad_maximum_fusion.2), channel_id=1, source_target_pairs={{0,16},{16,32},{32,48},{48,64},{64,80},{80,96},{96,112},{112,128},... | collective-permute-start | bytes 98312 | tf_op jit(solution)/shard_map/ppermute | solution.py:21
  13.2 29.0 %copy-start.1 = (bf16[512,192]{0,1:T(8,128)(2,1)S(1)}, bf16[512,192]{0,1:T(8,128)(2,1)}, u32[]{:S(2)}) copy-start(bf16[512,192]{0,1:T(8,128)(2,1)} %param.14) | copy-start | bytes 589828
  42.4 66.4 %copy-start.3 = (bf16[512,64]{0,1:T(8,128)(2,1)S(1)}, bf16[512,64]{0,1:T(8,128)(2,1)}, u32[]{:S(2)}) copy-start(bf16[512,64]{0,1:T(8,128)(2,1)} %param.16) | copy-start | bytes 196612
  108.8 2.2 %copy-start.6 = (f32[3,64]{1,0:T(4,128)S(1)}, f32[3,64]{1,0:T(4,128)}, u32[]{:S(2)}) copy-start(f32[3,64]{1,0:T(4,128)} %param.17) | copy-start | bytes 2308
  109.1 2.5 %copy-start.5 = (f32[3]{0:T(128)S(1)}, f32[3]{0:T(128)}, u32[]{:S(2)}) copy-start(f32[3]{0:T(128)} %param.19) | copy-start | bytes 40

commit v3 on v0

--- a/solution.py
+++ b/solution.py
@@ -1,6 +1,8 @@
 import jax
 import jax.numpy as jnp
 from jax import lax
+from jax.experimental import pallas as pl
+from jax.experimental.pallas import tpu as pltpu
 from jax.sharding import PartitionSpec as P
 
 EXPERTS = 32
@@ -98,12 +100,377 @@
     return jnp.einsum("rke,rkc,rk->rec", expert_hot, place_hot, route_weight)
 
 
-def expert_hidden(piece, gate_weight, up_weight):
-    gate_pre = jnp.einsum("aecd,edf->aecf", piece, gate_weight, preferred_element_type=jnp.float32)
-    up_pre = jnp.einsum("aecd,edf->aecf", piece, up_weight, preferred_element_type=jnp.float32)
-    clipped = jnp.minimum(gate_pre, CLAMP_LIMIT)
-    linear = jnp.clip(up_pre, -CLAMP_LIMIT, CLAMP_LIMIT)
-    return (clipped * jax.nn.sigmoid(ACT_SLOPE * clipped) * (linear + 1.0)).astype(jnp.bfloat16)
+CHAINS = ((0, 1, 4), (1, -1, 4), (1, 1, 3), (0, -1, 3))
+HOPS = {}
+for _half, _way, _far in CHAINS:
+    for _hop in range(1, _far + 1):
+        HOPS[_half, _way, _hop] = len(HOPS)
+X_RING = 4
+GROUPS = 2
+LANES = 128
+VMEM_LIMIT = 60 * 1024 * 1024
+
+
+def remote(source, target, send_sem, recv_sem, where):
+    return pltpu.make_async_remote_copy(
+        src_ref=source,
+        dst_ref=target,
+        send_sem=send_sem,
+        recv_sem=recv_sem,
+        device_id=where,
+        device_id_type=pl.DeviceIdType.MESH,
+    )
+
+
+def greet(places):
+    barrier = pltpu.get_barrier_semaphore()
+    for place in places:
+        pl.semaphore_signal(
+            barrier, inc=1, device_id=place, device_id_type=pl.DeviceIdType.MESH
+        )
+    pl.semaphore_wait(barrier, len(places))
+
+
+def exchange_order(count):
+    long = count // X_RING
+    order = [(0, across) for across in (0, 1, X_RING - 1, 2)]
+    for level in range(1, long // 2):
+        for across in (0, 1, X_RING - 1, 2):
+            order += [(level, across), (long - level, across)]
+    return order + [(long // 2, across) for across in (0, 1, X_RING - 1, 2)]
+
+
+def ep_place(me, offset, sign=1):
+    across_count = X_RING
+    along_count = lax.axis_size("ep") // X_RING
+    z, x = lax.div(me, across_count), lax.rem(me, across_count)
+    along = (sign * offset[0]) % along_count
+    across = (sign * offset[1]) % across_count
+    return lax.rem(z + along, along_count) * across_count + lax.rem(x + across, across_count)
+
+
+def layer_kernel(
+    x_ref,
+    gate_ref,
+    up_ref,
+    down_ref,
+    part_ref,
+    back_ref,
+    attended_ref,
+    w1,
+    w2,
+    abuf,
+    turn,
+    xbuf,
+    pbuf,
+    rbuf,
+    sbuf,
+    swapped,
+    pair,
+    prbuf,
+    wl_sem,
+    ws_sem,
+    wr_sem,
+    es_sem,
+    er_sem,
+    bs_sem,
+    br_sem,
+    gs_sem,
+    gr_sem,
+    ss_sem,
+    sr_sem,
+    swap_sem,
+    ps_sem,
+    pr_sem,
+):
+    me = lax.axis_index("ep")
+    count = lax.axis_size("ep")
+    tp = lax.axis_index("tp")
+    ring = lax.axis_size("tp") // 2
+    core, spot = lax.rem(tp, 2), lax.div(tp, 2)
+    ahead = {"tp": lax.rem(spot + 1, ring) * 2 + core}
+    behind = {"tp": lax.rem(spot + ring - 1, ring) * 2 + core}
+    partner = {"tp": spot * 2 + (1 - core)}
+    order = exchange_order(count)
+    inner = down_ref.shape[1]
+    members = count // GROUPS
+    rows, width = xbuf.shape[2], xbuf.shape[3]
+    strip = width // LANES
+
+    local = [
+        pltpu.make_async_copy(gate_ref.at[0], w1.at[:, pl.ds(0, inner)], wl_sem.at[0]),
+        pltpu.make_async_copy(up_ref.at[0], w1.at[:, pl.ds(2 * inner, inner)], wl_sem.at[1]),
+        pltpu.make_async_copy(down_ref.at[0], w2.at[pl.ds(0, inner)], wl_sem.at[2]),
+    ]
+    for copy in local:
+        copy.start()
+    greet(
+        [ahead, behind, partner] + [{"ep": ep_place(me, offset)} for offset in order[1:]]
+    )
+
+    def out_copy(number):
+        peer = ep_place(me, order[number])
+        return remote(
+            x_ref.at[peer], abuf.at[number], es_sem.at[number], er_sem.at[number], {"ep": peer}
+        )
+
+    def back_copy(number):
+        peer = ep_place(me, order[number], -1)
+        return remote(
+            sbuf.at[number], back_ref.at[me], bs_sem.at[number], br_sem.at[number], {"ep": peer}
+        )
+
+    def half_columns(half):
+        return pl.ds(half * (width // 2), width // 2)
+
+    def toward(way):
+        return ahead if way == 1 else behind
+
+    def gather_copy(group, half, way, hop):
+        number = HOPS[half, way, hop]
+        return remote(
+            xbuf.at[group, (-way * (hop - 1)) % ring, :, half_columns(half)],
+            xbuf.at[group, (-way * hop) % ring, :, half_columns(half)],
+            gs_sem.at[group, number],
+            gr_sem.at[group, number],
+            toward(way),
+        )
+
+    def sum_copy(group, half, way, hop):
+        number = HOPS[half, way, hop]
+        return remote(
+            pbuf.at[group, (way * hop) % ring, :, half_columns(half)],
+            rbuf.at[group, number],
+            ss_sem.at[group, number],
+            sr_sem.at[group, number],
+            toward(way),
+        )
+
+    def pair_copy(half, way, hop):
+        number = HOPS[half, way, hop]
+        return remote(
+            pair.at[(way * hop) % ring, :, half_columns(half)],
+            prbuf.at[number],
+            ps_sem.at[number],
+            pr_sem.at[number],
+            toward(way),
+        )
+
+    def running(buffer, received, copy_of, left):
+        for half, way, far in CHAINS:
+            hop = far - 3 + left
+            if hop < 1:
+                continue
+            copy_of(half, way, hop).wait_recv()
+            if hop > 1:
+                slot = (way * (hop - 1)) % ring
+                at = half_columns(half)
+                buffer[slot, :, at] = (
+                    buffer[slot, :, at].astype(jnp.float32)
+                    + received[HOPS[half, way, hop]].astype(jnp.float32)
+                ).astype(jnp.bfloat16)
+                copy_of(half, way, hop - 1).start()
+
+    def summed(buffer, received, half):
+        return (
+            buffer[0, :, half_columns(half)].astype(jnp.float32)
+            + received[HOPS[half, 1, 1]].astype(jnp.float32)
+            + received[HOPS[half, -1, 1]].astype(jnp.float32)
+        )
+
+    def experts(group, slot):
+        pre = jnp.dot(xbuf[group, slot], w1[...], preferred_element_type=jnp.float32)
+        clipped = jnp.minimum(pre[:, : 2 * inner], CLAMP_LIMIT)
+        linear = jnp.clip(pre[:, 2 * inner :], -CLAMP_LIMIT, CLAMP_LIMIT)
+        hidden = (clipped * jax.nn.sigmoid(ACT_SLOPE * clipped) * (linear + 1.0)).astype(
+            jnp.bfloat16
+        )
+        step = width // 4
+        for at in range(0, width, step):
+            pbuf[group, slot, :, at : at + step] = jnp.dot(
+                hidden, w2[:, at : at + step], preferred_element_type=jnp.float32
+            ).astype(jnp.bfloat16)
+
+    def arrive(group):
+        for number in range(group * members, (group + 1) * members):
+            if number > 0:
+                out_copy(number).wait_recv()
+        messages = abuf[group * members : (group + 1) * members]
+        turn[...] = messages.astype(jnp.float32).reshape(turn.shape)
+        for at in range(strip):
+            xbuf[group, 0, :, at * LANES : (at + 1) * LANES] = turn[
+                pl.ds(at, rows, stride=strip), :
+            ].astype(jnp.bfloat16)
+        for half, way, far in CHAINS:
+            gather_copy(group, half, way, 1).start()
+
+    def gather(group, hop):
+        for half, way, far in CHAINS:
+            if hop <= far:
+                gather_copy(group, half, way, hop).wait_recv()
+                if hop < far:
+                    gather_copy(group, half, way, hop + 1).start()
+        if hop < 4:
+
+            def both(index, carry):
+                experts(group, hop + index * (ring - 2 * hop))
+                return carry
+
+            lax.fori_loop(0, 2, both, 0)
+        else:
+            experts(group, 4)
+        for half, way, far in CHAINS:
+            if far == hop:
+                sum_copy(group, half, way, far).start()
+
+    def collect(group, left):
+        running(
+            pbuf.at[group],
+            rbuf.at[group],
+            lambda half, way, hop: sum_copy(group, half, way, hop),
+            left,
+        )
+
+    def give_back(group):
+        for half in range(2):
+            total = summed(pbuf.at[group], rbuf.at[group], half)
+            for at in range(strip // 2):
+                turn[pl.ds(half * (strip // 2) + at, rows, stride=strip), :] = total[
+                    :, at * LANES : (at + 1) * LANES
+                ]
+        sbuf[group * members : (group + 1) * members] = (
+            turn[...].reshape(members, -1, LANES).astype(jnp.bfloat16)
+        )
+        for number in range(group * members, (group + 1) * members):
+            if number > 0:
+                back_copy(number).start()
+
+    for number in range(1, count):
+        out_copy(number).start()
+    swap = remote(part_ref.at[:, 1 - core], swapped, swap_sem.at[0], swap_sem.at[1], partner)
+    swap.start()
+    shared = [
+        remote(
+            gate_ref.at[0], w1.at[:, pl.ds(inner, inner)], ws_sem.at[0], wr_sem.at[0], partner
+        ),
+        remote(
+            up_ref.at[0], w1.at[:, pl.ds(3 * inner, inner)], ws_sem.at[1], wr_sem.at[1], partner
+        ),
+        remote(down_ref.at[0], w2.at[pl.ds(inner, inner)], ws_sem.at[2], wr_sem.at[2], partner),
+    ]
+    for copy in shared:
+        copy.start()
+    abuf[0] = x_ref[me]
+    swap.wait_recv()
+    for slot in (4, 3, 5, 2, 6, 1, 7, 0):
+        owner = lax.rem(spot + slot, ring)
+        pair[slot] = (
+            part_ref[owner, core].astype(jnp.float32) + swapped[owner].astype(jnp.float32)
+        ).astype(jnp.bfloat16)
+        for half, way, far in CHAINS:
+            if (way * far) % ring == slot:
+                pair_copy(half, way, far).start()
+    running(pair, prbuf, pair_copy, 3)
+    running(pair, prbuf, pair_copy, 2)
+    arrive(0)
+    for copy in local:
+        copy.wait()
+    for copy in shared:
+        copy.wait_recv()
+    experts(0, 0)
+    running(pair, prbuf, pair_copy, 1)
+    gather(0, 1)
+    running(pair, prbuf, pair_copy, 0)
+    for half in range(2):
+        attended_ref[:, half_columns(half)] = summed(pair, prbuf, half).astype(jnp.bfloat16)
+    arrive(1)
+    gather(0, 2)
+    experts(1, 0)
+    gather(1, 1)
+    gather(0, 3)
+    gather(1, 2)
+    gather(0, 4)
+    gather(1, 3)
+    collect(0, 3)
+    gather(1, 4)
+    collect(0, 2)
+    collect(1, 3)
+    collect(0, 1)
+    collect(1, 2)
+    collect(0, 0)
+    give_back(0)
+    collect(1, 1)
+    collect(1, 0)
+    give_back(1)
+    back_ref[me] = sbuf[0]
+    swap.wait_send()
+    for copy in shared:
+        copy.wait_send()
+    for half, way, hop in HOPS:
+        pair_copy(half, way, hop).wait_send()
+        for group in range(GROUPS):
+            gather_copy(group, half, way, hop).wait_send()
+            sum_copy(group, half, way, hop).wait_send()
+    for number in range(1, count):
+        out_copy(number).wait_send()
+        back_copy(number).wait()
+
+
+def layer(messages, gate_weight, up_weight, down_weight, partial_rows):
+    count = messages.shape[0]
+    width = gate_weight.shape[1]
+    inner = down_weight.shape[1]
+    ring = lax.axis_size("tp") // 2
+    own = partial_rows.shape[0] // (2 * ring)
+    rows = messages.size // width // GROUPS
+    hops = len(HOPS)
+    dma = pltpu.SemaphoreType.DMA
+
+    def scratch(*shape):
+        return pltpu.VMEM(shape, jnp.bfloat16)
+
+    return pl.pallas_call(
+        layer_kernel,
+        out_shape=(
+            jax.ShapeDtypeStruct(messages.shape, messages.dtype),
+            jax.ShapeDtypeStruct((own, width), jnp.bfloat16),
+        ),
+        in_specs=[pl.BlockSpec(memory_space=pltpu.VMEM)]
+        + [pl.BlockSpec(memory_space=pl.ANY)] * 3
+        + [pl.BlockSpec(memory_space=pltpu.VMEM)],
+        out_specs=[pl.BlockSpec(memory_space=pltpu.VMEM)] * 2,
+        scratch_shapes=[
+            scratch(width, 4 * inner),
+            scratch(2 * inner, width),
+            scratch(*messages.shape),
+            pltpu.VMEM((messages.size // LANES // GROUPS, LANES), jnp.float32),
+            scratch(GROUPS, ring, rows, width),
+            scratch(GROUPS, ring, rows, width),
+            scratch(GROUPS, hops, rows, width // 2),
+            scratch(*messages.shape),
+            scratch(ring, own, width),
+            scratch(ring, own, width),
+            scratch(hops, own, width // 2),
+            dma((3,)),
+            dma((3,)),
+            dma((3,)),
+            dma((count,)),
+            dma((count,)),
+            dma((count,)),
+            dma((count,)),
+            dma((GROUPS, hops)),
+            dma((GROUPS, hops)),
+            dma((GROUPS, hops)),
+            dma((GROUPS, hops)),
+            dma((2,)),
+            dma((hops,)),
+            dma((hops,)),
+        ],
+        compiler_params=pltpu.CompilerParams(
+            collective_id=1, has_side_effects=True, vmem_limit_bytes=VMEM_LIMIT
+        ),
+        name="layer",
+    )(messages, gate_weight, up_weight, down_weight, partial_rows.reshape(ring, 2, own, width))
 
 
 def on_device(
@@ -123,18 +490,13 @@
     down_weight,
 ):
     heads_out = attend(query_rows, key_rows, value_rows, query_gain, key_gain, sink_logits)
-    attended = lax.psum_scatter(
-        jnp.dot(heads_out, out_weight, preferred_element_type=jnp.float32).astype(jnp.bfloat16),
-        "tp",
-        scatter_dimension=0,
-        tiled=True,
+    partial_rows = jnp.dot(heads_out, out_weight, preferred_element_type=jnp.float32).astype(
+        jnp.bfloat16
     )
     own_rows = expert_input.shape[0]
     fanout = routes.shape[1]
     capacity = (3 * own_rows * fanout + 2 * EXPERTS - 1) // (2 * EXPERTS)
     ep_size = lax.axis_size("ep")
-    tp_size = lax.axis_size("tp")
-    local_experts = gate_weight.shape[0]
     widened = expert_input.astype(jnp.float32)
     normed = (
         widened
@@ -147,19 +509,9 @@
     slot_rows = jnp.einsum(
         "ecr,rd->ecd", sender, normed, preferred_element_type=jnp.float32
     ).astype(jnp.bfloat16)
-    slot_rows = slot_rows.reshape(ep_size, local_experts, capacity, -1)
-    arrived = lax.all_to_all(slot_rows, "ep", split_axis=0, concat_axis=0, tiled=True)
-    hidden_units = expert_hidden(
-        lax.all_gather(arrived, "tp", axis=0, tiled=True), gate_weight, up_weight
-    )
-    partial_value = jnp.einsum(
-        "aecf,efd->aecd", hidden_units, down_weight, preferred_element_type=jnp.float32
-    ).astype(jnp.bfloat16)
-    partial_value = partial_value.reshape(tp_size, ep_size * local_experts * capacity, -1)
-    pieces = lax.all_to_all(partial_value, "tp", split_axis=0, concat_axis=0, tiled=True)
-    summed = jnp.sum(pieces, axis=0, dtype=jnp.float32).astype(jnp.bfloat16)
-    summed = summed.reshape(ep_size, local_experts * capacity, -1)
-    returned = lax.all_to_all(summed, "ep", split_axis=0, concat_axis=0, tiled=True)
+    messages = slot_rows.reshape(ep_size, -1, 128)
+    returned, attended = layer(messages, gate_weight, up_weight, down_weight, partial_rows)
+    returned = returned.reshape(EXPERTS, capacity, -1)
     expert_mix = jnp.einsum("rec,ecd->rd", combine, returned.astype(jnp.float32)).astype(
         jnp.bfloat16
     )

time: 329 us -> 127 us (0.39)
  the two profiles are of different devices: /device:TPU:24 before, /device:TPU:8 now
where the time goes in v3:
time: 127 us
  Pallas kernels  104 us (82%)
  other arithmetic  7.03 us (6%)
  local copies, waits for them, and re-layouts  6.85 us (5%)
  matrix products  5.07 us (4%)
  starting transfers between devices  3.4 us (3%)
    pallas_call x1, Pallas kernels, layer(): pl.pallas_call(layer_kernel, out_shape=(jax.ShapeDtypeStruct(messages.sha...  104 us
    ppermute x1, starting transfers between devices, shifted(): lax.ppermute(value, axis, [(source, source + steps) for source in range(i...  3.4 us
  transfers between devices with their start and end apart: 1, of which 0 were waited for; matrix products, arithmetic and copies ran while one was open for 7% of the time, Pallas kernels for 0%

profile of v3, /device:TPU:8, one launch (start us, length us, event | category | flops | bytes accessed | tf_op | source)
XLA Modules:
  0.0 127.1 jit_solution(6402605681929940136)
XLA Ops:
  0.7 1.0 fusion.19
  1.6 0.9 fusion.21
  2.6 0.8 slice_bitcast_fusion.2
  3.3 3.4 %collective-permute-start = (bf16[2,128,1,64]{1,3,2,0:T(8,128)(2,1)S(1)}, bf16[2,128,1,64]{1,3,2,0:T(8,128)(2,1)S(1)}, u32[]{:S(2)}, u32[]{:S(2)}) collective-permute-start(bf16[2,128,1,64]{1,3,2,0:T(8,128)(2,1)S(1)} %pad_maximum_fusion.2), channel_id=1, source_target_pairs={{0,16},{16,32},{32,48},{48,64},{64,80},{80,96},{96,112},{112,128},... | collective-permute-start | bytes 98312 | tf_op jit(solution)/shard_map/ppermute | solution.py:21
  6.8 0.9 fusion.58
  7.7 0.7 reduce_max.19
  8.4 0.7 fusion.52
  9.1 0.7 fusion.51
  9.8 1.0 fusion.11
  11.0 0.8 copy.23
  12.1 0.2 select_reduce_fusion
  12.4 0.4 fusion.40
  12.7 0.4 fusion.37
  13.5 0.3 convolution_convert_fusion.1
  14.1 0.3 copy.25
  14.5 1.2 reshape.185.x_ref
  15.7 0.5 fusion.56
  16.3 0.2 fusion.1
  16.6 0.4 fusion.4
  17.1 2.1 %convolution_convert_fusion = bf16[512,2048]{1,0:T(8,128)(2,1)} fusion(bf16[192,2048]{1,0:T(8,128)(2,1)S(1)} %copy-done, bf16[24,8,4,128]{3,2,1,0:T(4,128)(2,1)S(1)} %bitcast.77), kind=kOutput, calls=%fused_computation | convolution fusion | flops 403701760 | bytes 3080192 | tf_op jit(solution)/shard_map/dot_general | solution.py:493
  19.2 103.8 %layer.1 = (bf16[32,48,128]{2,1,0:T(8,128)(2,1)}, bf16[32,2048]{1,0:T(8,128)(2,1)}) custom-call(bf16[32,48,128]{2,1,0:T(8,128)(2,1)} %reshape.185.x_ref, bf16[1,2048,128]{2,1,0:T(8,128)(2,1)} %gate_ref.1, bf16[1,2048,128]{2,1,0:T(8,128)(2,1)} %up_ref.1, bf16[1,128,2048]{2,1,0:T(8,128)(2,1)} %down_ref.1, bf16[8,2,32,2048]{3,2,1,0:T(8,128)(2,1)} %bitcast.75), custom_call_target="tpu_custom_call" | custom-call | tf_op jit(solution)/shard_map/layer/pallas_call | solution.py:432
  123.0 1.4 %reshape.193 = bf16[32,3,2048]{2,1,0:T(4,128)(2,1)S(1)} reshape(bf16[32,48,128]{2,1,0:T(8,128)(2,1)} %get-tuple-element.5) | data formatting | bytes 786432 | tf_op jit(solution)/shard_map/reshape | solution.py:514
  124.4 1.1 fusion
  125.5 1.6 %copy.63 = bf16[32,2048]{1,0:T(8,128)(2,1)} copy(bf16[32,2048]{1,0:T(8,128)(2,1)} %get-tuple-element.14) | data formatting | bytes 262144
  (43 shorter events, 1.5 us)
Async XLA Ops:
  0.6 16.5 %copy-start = (bf16[192,2048]{1,0:T(8,128)(2,1)S(1)}, bf16[192,2048]{1,0:T(8,128)(2,1)}, u32[]{:S(2)}) copy-start(bf16[192,2048]{1,0:T(8,128)(2,1)} %param.20) | copy-start | bytes 2359300
  0.6 12.6 %copy-start.1 = (bf16[512,192]{0,1:T(8,128)(2,1)S(1)}, bf16[512,192]{0,1:T(8,128)(2,1)}, u32[]{:S(2)}) copy-start(bf16[512,192]{0,1:T(8,128)(2,1)} %param.14) | copy-start | bytes 589828
  2.6 10.9 %copy-start.2 = (bf16[32,2048]{1,0:T(8,128)(2,1)S(1)}, bf16[32,2048]{1,0:T(8,128)(2,1)}, u32[]{:S(2)}) copy-start(bf16[32,2048]{1,0:T(8,128)(2,1)} %param.21) | copy-start | bytes 393220
  2.6 10.9 %copy-start.4 = (f32[2048]{0:T(1024)S(1)}, f32[2048]{0:T(1024)}, u32[]{:S(2)}) copy-start(f32[2048]{0:T(1024)} %param.22) | copy-start | bytes 24580
  3.3 12.3 %collective-permute-start = (bf16[2,128,1,64]{1,3,2,0:T(8,128)(2,1)S(1)}, bf16[2,128,1,64]{1,3,2,0:T(8,128)(2,1)S(1)}, u32[]{:S(2)}, u32[]{:S(2)}) collective-permute-start(bf16[2,128,1,64]{1,3,2,0:T(8,128)(2,1)S(1)} %pad_maximum_fusion.2), channel_id=1, source_target_pairs={{0,16},{16,32},{32,48},{48,64},{64,80},{80,96},{96,112},{112,128},... | collective-permute-start | bytes 98312 | tf_op jit(solution)/shard_map/ppermute | solution.py:21
  12.4 1.5 %copy-start.3 = (bf16[512,64]{0,1:T(8,128)(2,1)S(1)}, bf16[512,64]{0,1:T(8,128)(2,1)}, u32[]{:S(2)}) copy-start(bf16[512,64]{0,1:T(8,128)(2,1)} %param.16) | copy-start | bytes 196612
  13.8 1.8 %copy-start.6 = (f32[3,64]{1,0:T(4,128)S(1)}, f32[3,64]{1,0:T(4,128)}, u32[]{:S(2)}) copy-start(f32[3,64]{1,0:T(4,128)} %param.17) | copy-start | bytes 2308
  14.4 1.7 %copy-start.5 = (f32[3]{0:T(128)S(1)}, f32[3]{0:T(128)}, u32[]{:S(2)}) copy-start(f32[3]{0:T(128)} %param.19) | copy-start | bytes 40

commit v4 on v3

--- a/solution.py
+++ b/solution.py
@@ -5,101 +5,11 @@
 from jax.experimental.pallas import tpu as pltpu
 from jax.sharding import PartitionSpec as P
 
-EXPERTS = 32
 WINDOW = 128
-
-
 EPSILON = 1e-06
 CLAMP_LIMIT = 7.0
 ACT_SLOPE = 1.702
 NEGATIVE = -1e30
-
-
-def shifted(value, axis, steps):
-    count = lax.axis_size(axis)
-    initial, last = (max(0, -steps), min(count, count - steps))
-    return lax.ppermute(value, axis, [(source, source + steps) for source in range(initial, last)])
-
-
-def head_norm(row_data, gain_table):
-    head_count, head_size = gain_table.shape
-    widened = row_data.astype(jnp.float32).reshape(row_data.shape[0], head_count, head_size)
-    scaled = widened * lax.rsqrt(jnp.mean(widened * widened, axis=-1, keepdims=True) + EPSILON)
-    return (scaled * gain_table).astype(jnp.bfloat16)
-
-
-def band(padded, blocks):
-    tiled = padded.reshape((blocks + 1, WINDOW) + padded.shape[1:])
-    return jnp.concatenate([tiled[:-1], tiled[1:]], axis=1)
-
-
-def attend(query_rows, key_rows, value_rows, query_gain, key_gain, sink_logits):
-    seq_rows = query_rows.shape[0]
-    key_heads, head_size = key_gain.shape
-    group_size = query_gain.shape[0] // key_heads
-    blocks = seq_rows // WINDOW
-    query_hat = head_norm(query_rows, query_gain).reshape(
-        blocks, WINDOW, key_heads, group_size, head_size
-    )
-    key_hat = head_norm(key_rows, key_gain)
-    value_hat = value_rows.reshape(seq_rows, key_heads, head_size)
-    tail_rows = jnp.stack([key_hat[seq_rows - WINDOW :], value_hat[seq_rows - WINDOW :]])
-    earlier = shifted(tail_rows, "ep", 1)
-    key_band = band(jnp.concatenate([earlier[0], key_hat], axis=0), blocks)
-    value_band = band(jnp.concatenate([earlier[1], value_hat], axis=0), blocks)
-    query_pos = lax.broadcasted_iota(jnp.int32, (WINDOW, 2 * WINDOW), 0)
-    key_pos = lax.broadcasted_iota(jnp.int32, (WINDOW, 2 * WINDOW), 1)
-    distance = query_pos + WINDOW - key_pos
-    inside = (distance >= 0) & (distance < WINDOW)
-    first_block = (lax.broadcasted_iota(jnp.int32, (blocks, 1, 1), 0) == 0) & (
-        lax.axis_index("ep") == 0
-    )
-    allowed = inside[None] & ~(first_block & (key_pos < WINDOW)[None])
-    scores = jnp.einsum(
-        "bqkgd,bjkd->bkgqj", query_hat, key_band, preferred_element_type=jnp.float32
-    ) * head_size ** (-0.5)
-    scores = jnp.where(allowed[:, None, None], scores, NEGATIVE)
-    sink_table = sink_logits.reshape(1, key_heads, group_size, 1, 1)
-    highest = jnp.maximum(jnp.max(scores, axis=-1, keepdims=True), sink_table)
-    weights = jnp.exp(scores - highest)
-    total = jnp.sum(weights, axis=-1, keepdims=True) + jnp.exp(sink_table - highest)
-    mixed = jnp.einsum(
-        "bkgqj,bjkd->bkgqd",
-        weights.astype(jnp.bfloat16),
-        value_band,
-        preferred_element_type=jnp.float32,
-    )
-    mixed = (mixed / total).astype(jnp.bfloat16)
-    return jnp.transpose(mixed, (0, 3, 1, 2, 4)).reshape(seq_rows, -1)
-
-
-def slot_maps(route_block, capacity):
-    flat_routes = route_block.reshape(-1)
-    expert_hot = (flat_routes[:, None] == lax.broadcasted_iota(jnp.int32, (1, EXPERTS), 1)).astype(
-        jnp.int32
-    )
-    before = jnp.cumsum(expert_hot, axis=0) - expert_hot
-    position = jnp.sum(before * expert_hot, axis=1)
-    place_hot = (position[:, None] == lax.broadcasted_iota(jnp.int32, (1, capacity), 1)).astype(
-        jnp.float32
-    )
-    row_total, fanout = route_block.shape
-    return (
-        expert_hot.astype(jnp.float32).reshape(row_total, fanout, EXPERTS),
-        place_hot.reshape(row_total, fanout, capacity),
-    )
-
-
-def dispatch_matrix(route_block, capacity):
-    expert_hot, place_hot = slot_maps(route_block, capacity)
-    return jnp.einsum("rke,rkc->ecr", expert_hot, place_hot).astype(jnp.bfloat16)
-
-
-def combine_matrix(route_block, route_weight, capacity):
-    expert_hot, place_hot = slot_maps(route_block, capacity)
-    return jnp.einsum("rke,rkc,rk->rec", expert_hot, place_hot, route_weight)
-
-
 CHAINS = ((0, 1, 4), (1, -1, 4), (1, 1, 3), (0, -1, 3))
 HOPS = {}
 for _half, _way, _far in CHAINS:
@@ -122,13 +32,25 @@
     )
 
 
-def greet(places):
-    barrier = pltpu.get_barrier_semaphore()
-    for place in places:
-        pl.semaphore_signal(
-            barrier, inc=1, device_id=place, device_id_type=pl.DeviceIdType.MESH
-        )
-    pl.semaphore_wait(barrier, len(places))
+def column(row):
+    size = row.shape[1]
+    square = (size, size)
+    diagonal = lax.broadcasted_iota(jnp.int32, square, 0) == lax.broadcasted_iota(
+        jnp.int32, square, 1
+    )
+    return jnp.sum(jnp.where(diagonal, jnp.broadcast_to(row, square), 0.0), axis=1, keepdims=True)
+
+
+def head_norm(rows, gain_row):
+    widened = rows.astype(jnp.float32)
+    scaled = widened * lax.rsqrt(jnp.mean(widened * widened, axis=0, keepdims=True) + EPSILON)
+    return (scaled * column(gain_row)).astype(jnp.bfloat16)
+
+
+def contract_rows(left, right):
+    return lax.dot_general(
+        left, right, (((0,), (0,)), ((), ())), preferred_element_type=jnp.float32
+    )
 
 
 def exchange_order(count):
@@ -150,13 +72,29 @@
 
 
 def layer_kernel(
-    x_ref,
+    query_ref,
+    key_ref,
+    value_ref,
+    query_gain_ref,
+    key_gain_ref,
+    sink_ref,
+    project_ref,
+    input_ref,
+    input_gain_ref,
+    routes_ref,
+    logits_ref,
     gate_ref,
     up_ref,
     down_ref,
+    attended_ref,
+    mix_ref,
+    x_ref,
+    back_ref,
+    keys,
+    values,
+    queries,
+    heads,
     part_ref,
-    back_ref,
-    attended_ref,
     w1,
     w2,
     abuf,
@@ -182,6 +120,8 @@
     swap_sem,
     ps_sem,
     pr_sem,
+    hs_sem,
+    hr_sem,
 ):
     me = lax.axis_index("ep")
     count = lax.axis_size("ep")
@@ -204,9 +144,12 @@
     ]
     for copy in local:
         copy.start()
-    greet(
-        [ahead, behind, partner] + [{"ep": ep_place(me, offset)} for offset in order[1:]]
-    )
+    peers = [ahead, behind, partner] + [{"ep": ep_place(me, offset)} for offset in order[1:]]
+    barrier = pltpu.get_barrier_semaphore()
+    for place in peers:
+        pl.semaphore_signal(
+            barrier, inc=1, device_id=place, device_id_type=pl.DeviceIdType.MESH
+        )
 
     def out_copy(number):
         peer = ep_place(me, order[number])
@@ -296,7 +239,7 @@
             if number > 0:
                 out_copy(number).wait_recv()
         messages = abuf[group * members : (group + 1) * members]
-        turn[...] = messages.astype(jnp.float32).reshape(turn.shape)
+        turn[: rows * strip] = messages.astype(jnp.float32).reshape(rows * strip, LANES)
         for at in range(strip):
             xbuf[group, 0, :, at * LANES : (at + 1) * LANES] = turn[
                 pl.ds(at, rows, stride=strip), :
@@ -339,16 +282,79 @@
                     :, at * LANES : (at + 1) * LANES
                 ]
         sbuf[group * members : (group + 1) * members] = (
-            turn[...].reshape(members, -1, LANES).astype(jnp.bfloat16)
+            turn[: rows * strip].reshape(members, -1, LANES).astype(jnp.bfloat16)
         )
         for number in range(group * members, (group + 1) * members):
             if number > 0:
                 back_copy(number).start()
 
+    head_size = key_ref.shape[0]
+    group_heads = query_ref.shape[0] // head_size
+    seq_rows = key_ref.shape[1]
+    blocks = seq_rows // WINDOW
+    slots = count * x_ref.shape[1] // strip
+    capacity = x_ref.shape[1] // strip
+    tokens = input_ref.shape[0]
+
+    keys[:, WINDOW:] = head_norm(key_ref[...], key_gain_ref[...])
+    values[:, WINDOW:] = value_ref[...]
+
+    given = input_ref[...].astype(jnp.float32)
+    normed = (
+        given
+        * lax.rsqrt(jnp.mean(given * given, axis=-1, keepdims=True) + EPSILON)
+        * input_gain_ref[...]
+    ).astype(jnp.bfloat16)
+    place = lax.broadcasted_iota(jnp.int32, (slots, tokens), 0)
+    offset = [place - capacity * routes_ref[copy : copy + 1, :] for copy in range(2)]
+    named = [(gap >= 0) & (gap < capacity) for gap in offset]
+    hot = [jnp.where(flag, 1.0, 0.0) for flag in named]
+    square = (tokens, tokens)
+    before = jnp.where(
+        lax.broadcasted_iota(jnp.int32, square, 0) < lax.broadcasted_iota(jnp.int32, square, 1),
+        1.0,
+        0.0,
+    ).astype(jnp.bfloat16)
+    taken = jnp.dot(
+        (hot[0] + hot[1]).astype(jnp.bfloat16), before, preferred_element_type=jnp.float32
+    )
+    picked = [
+        jnp.where(flag & (taken == gap.astype(jnp.float32)), 1.0, 0.0)
+        for flag, gap in zip(named, offset)
+    ]
+    logits = logits_ref[...]
+    top_logit = jnp.max(logits, axis=0, keepdims=True)
+    raised = jnp.exp(logits - top_logit)
+    share = raised / jnp.sum(raised, axis=0, keepdims=True)
+    weighted = picked[0] * share[0:1, :] + picked[1] * share[1:2, :]
+    coarse = weighted.astype(jnp.bfloat16)
+    fine = (weighted - coarse.astype(jnp.float32)).astype(jnp.bfloat16)
+    sender = (picked[0] + picked[1]).astype(jnp.bfloat16)
+    step = width // 4
+    for at in range(0, width, step):
+        slot_rows = jnp.dot(sender, normed[:, at : at + step], preferred_element_type=jnp.float32)
+        for lane in range(0, step, LANES):
+            turn[pl.ds((at + lane) // LANES, slots, stride=strip), :] = slot_rows[
+                :, lane : lane + LANES
+            ]
+    x_ref[...] = turn[...].reshape(x_ref.shape).astype(jnp.bfloat16)
+
+    pl.semaphore_wait(barrier, len(peers))
+    following = {"ep": lax.rem(me + 1, count)}
+    halo = [
+        remote(
+            buffer.at[:, pl.ds(seq_rows, WINDOW)],
+            buffer.at[:, pl.ds(0, WINDOW)],
+            hs_sem.at[index],
+            hr_sem.at[index],
+            following,
+        )
+        for index, buffer in enumerate((keys, values))
+    ]
+    for copy in halo:
+        copy.start()
     for number in range(1, count):
         out_copy(number).start()
-    swap = remote(part_ref.at[:, 1 - core], swapped, swap_sem.at[0], swap_sem.at[1], partner)
-    swap.start()
     shared = [
         remote(
             gate_ref.at[0], w1.at[:, pl.ds(inner, inner)], ws_sem.at[0], wr_sem.at[0], partner
@@ -361,6 +367,65 @@
     for copy in shared:
         copy.start()
     abuf[0] = x_ref[me]
+
+    for head in range(group_heads):
+        hat = head_norm(
+            query_ref[head * head_size : (head + 1) * head_size, :],
+            query_gain_ref[head : head + 1, :],
+        )
+        for block in range(blocks):
+            queries[block, :, head * WINDOW : (head + 1) * WINDOW] = hat[
+                :, block * WINDOW : (block + 1) * WINDOW
+            ]
+    band = (2 * WINDOW, WINDOW)
+    key_pos = lax.broadcasted_iota(jnp.int32, band, 0)
+    distance = lax.broadcasted_iota(jnp.int32, band, 1) + WINDOW - key_pos
+    inside = (distance >= 0) & (distance < WINDOW)
+    inside_first = inside & ((key_pos >= WINDOW) | (me > 0))
+
+    def attend(block):
+        at = pl.ds(block * WINDOW, 2 * WINDOW)
+        scores = contract_rows(keys[:, at], queries[block]) * head_size**-0.5
+        allowed = inside_first if block == 0 else inside
+        for head in range(group_heads):
+            lanes = slice(head * WINDOW, (head + 1) * WINDOW)
+            own = jnp.where(allowed, scores[:, lanes], NEGATIVE)
+            sink = jnp.full((1, WINDOW), sink_ref[0, head], jnp.float32)
+            highest = jnp.maximum(jnp.max(own, axis=0, keepdims=True), sink)
+            weights = jnp.exp(own - highest)
+            total = jnp.sum(weights, axis=0, keepdims=True) + jnp.exp(sink - highest)
+            mixed = jnp.dot(
+                values[:, at], weights.astype(jnp.bfloat16), preferred_element_type=jnp.float32
+            )
+            heads[head * head_size : (head + 1) * head_size, block * WINDOW : (block + 1) * WINDOW] = (
+                mixed / total
+            ).astype(jnp.bfloat16)
+
+    def project(block):
+        owners = WINDOW // tokens // 2
+        rows_in = heads[:, block * WINDOW : (block + 1) * WINDOW]
+        for at in range(0, width, step):
+            part_ref[block * owners : (block + 1) * owners, :, :, at : at + step] = (
+                contract_rows(rows_in, project_ref[:, at : at + step])
+                .astype(jnp.bfloat16)
+                .reshape(owners, 2, tokens, step)
+            )
+
+    for block in range(1, blocks):
+        attend(block)
+        project(block)
+    for copy in halo:
+        copy.wait_recv()
+    attend(0)
+    project(0)
+    swap = remote(part_ref.at[:, 1 - core], swapped, swap_sem.at[0], swap_sem.at[1], partner)
+    swap.start()
+    arrive(0)
+    for copy in local:
+        copy.wait()
+    for copy in shared:
+        copy.wait_recv()
+    experts(0, 0)
     swap.wait_recv()
     for slot in (4, 3, 5, 2, 6, 1, 7, 0):
         owner = lax.rem(spot + slot, ring)
@@ -370,26 +435,20 @@
         for half, way, far in CHAINS:
             if (way * far) % ring == slot:
                 pair_copy(half, way, far).start()
+    gather(0, 1)
+    arrive(1)
     running(pair, prbuf, pair_copy, 3)
+    gather(0, 2)
+    experts(1, 0)
     running(pair, prbuf, pair_copy, 2)
-    arrive(0)
-    for copy in local:
-        copy.wait()
-    for copy in shared:
-        copy.wait_recv()
-    experts(0, 0)
+    gather(1, 1)
+    gather(0, 3)
     running(pair, prbuf, pair_copy, 1)
-    gather(0, 1)
+    gather(1, 2)
+    gather(0, 4)
     running(pair, prbuf, pair_copy, 0)
     for half in range(2):
         attended_ref[:, half_columns(half)] = summed(pair, prbuf, half).astype(jnp.bfloat16)
-    arrive(1)
-    gather(0, 2)
-    experts(1, 0)
-    gather(1, 1)
-    gather(0, 3)
-    gather(1, 2)
-    gather(0, 4)
     gather(1, 3)
     collect(0, 3)
     gather(1, 4)
@@ -404,7 +463,7 @@
     give_back(1)
     back_ref[me] = sbuf[0]
     swap.wait_send()
-    for copy in shared:
+    for copy in shared + halo:
         copy.wait_send()
     for half, way, hop in HOPS:
         pair_copy(half, way, hop).wait_send()
@@ -414,40 +473,71 @@
     for number in range(1, count):
         out_copy(number).wait_send()
         back_copy(number).wait()
-
-
-def layer(messages, gate_weight, up_weight, down_weight, partial_rows):
-    count = messages.shape[0]
-    width = gate_weight.shape[1]
+    turn[...] = back_ref[...].astype(jnp.float32).reshape(turn.shape)
+    for at in range(strip):
+        came = turn[pl.ds(at, slots, stride=strip), :].astype(jnp.bfloat16)
+        mix_ref[:, at * LANES : (at + 1) * LANES] = (
+            contract_rows(coarse, came) + contract_rows(fine, came)
+        ).astype(jnp.bfloat16)
+
+
+def on_device(
+    query_rows,
+    key_rows,
+    value_rows,
+    query_gain,
+    key_gain,
+    sink_logits,
+    out_weight,
+    expert_input,
+    expert_gain,
+    routes,
+    route_logits,
+    gate_weight,
+    up_weight,
+    down_weight,
+):
+    own, width = expert_input.shape
+    fanout = routes.shape[1]
+    count = lax.axis_size("ep")
+    capacity = (3 * own * fanout + 2 * count - 1) // (2 * count)
     inner = down_weight.shape[1]
     ring = lax.axis_size("tp") // 2
-    own = partial_rows.shape[0] // (2 * ring)
-    rows = messages.size // width // GROUPS
+    rows = count * capacity // GROUPS
+    seq_rows, query_width = query_rows.shape
+    head_size = key_rows.shape[1]
+    message = (count, capacity * width // LANES, LANES)
     hops = len(HOPS)
     dma = pltpu.SemaphoreType.DMA
+    vmem = pl.BlockSpec(memory_space=pltpu.VMEM)
 
     def scratch(*shape):
         return pltpu.VMEM(shape, jnp.bfloat16)
 
     return pl.pallas_call(
         layer_kernel,
-        out_shape=(
-            jax.ShapeDtypeStruct(messages.shape, messages.dtype),
-            jax.ShapeDtypeStruct((own, width), jnp.bfloat16),
-        ),
-        in_specs=[pl.BlockSpec(memory_space=pltpu.VMEM)]
-        + [pl.BlockSpec(memory_space=pl.ANY)] * 3
-        + [pl.BlockSpec(memory_space=pltpu.VMEM)],
-        out_specs=[pl.BlockSpec(memory_space=pltpu.VMEM)] * 2,
+        out_shape=(jax.ShapeDtypeStruct((own, width), jnp.bfloat16),) * 2,
+        in_specs=[vmem] * 5
+        + [pl.BlockSpec(memory_space=pltpu.SMEM)]
+        + [vmem] * 5
+        + [pl.BlockSpec(memory_space=pl.ANY)] * 3,
+        out_specs=[vmem] * 2,
         scratch_shapes=[
+            scratch(*message),
+            scratch(*message),
+            scratch(head_size, seq_rows + WINDOW),
+            scratch(head_size, seq_rows + WINDOW),
+            scratch(seq_rows // WINDOW, head_size, query_width // head_size * WINDOW),
+            scratch(query_width, seq_rows),
+            scratch(ring, 2, own, width),
             scratch(width, 4 * inner),
             scratch(2 * inner, width),
-            scratch(*messages.shape),
-            pltpu.VMEM((messages.size // LANES // GROUPS, LANES), jnp.float32),
+            scratch(*message),
+            pltpu.VMEM((count * capacity * width // LANES, LANES), jnp.float32),
             scratch(GROUPS, ring, rows, width),
             scratch(GROUPS, ring, rows, width),
             scratch(GROUPS, hops, rows, width // 2),
-            scratch(*messages.shape),
+            scratch(*message),
             scratch(ring, own, width),
             scratch(ring, own, width),
             scratch(hops, own, width // 2),
@@ -465,57 +555,29 @@
             dma((2,)),
             dma((hops,)),
             dma((hops,)),
+            dma((2,)),
+            dma((2,)),
         ],
         compiler_params=pltpu.CompilerParams(
             collective_id=1, has_side_effects=True, vmem_limit_bytes=VMEM_LIMIT
         ),
         name="layer",
-    )(messages, gate_weight, up_weight, down_weight, partial_rows.reshape(ring, 2, own, width))
-
-
-def on_device(
-    query_rows,
-    key_rows,
-    value_rows,
-    query_gain,
-    key_gain,
-    sink_logits,
-    out_weight,
-    expert_input,
-    expert_gain,
-    routes,
-    route_logits,
-    gate_weight,
-    up_weight,
-    down_weight,
-):
-    heads_out = attend(query_rows, key_rows, value_rows, query_gain, key_gain, sink_logits)
-    partial_rows = jnp.dot(heads_out, out_weight, preferred_element_type=jnp.float32).astype(
-        jnp.bfloat16
+    )(
+        query_rows.T,
+        key_rows.T,
+        value_rows.T,
+        query_gain,
+        key_gain,
+        sink_logits.reshape(1, -1),
+        out_weight,
+        expert_input,
+        expert_gain.reshape(1, -1),
+        routes.T,
+        route_logits.T,
+        gate_weight,
+        up_weight,
+        down_weight,
     )
-    own_rows = expert_input.shape[0]
-    fanout = routes.shape[1]
-    capacity = (3 * own_rows * fanout + 2 * EXPERTS - 1) // (2 * EXPERTS)
-    ep_size = lax.axis_size("ep")
-    widened = expert_input.astype(jnp.float32)
-    normed = (
-        widened
-        * lax.rsqrt(jnp.mean(widened * widened, axis=-1, keepdims=True) + EPSILON)
-        * expert_gain
-    ).astype(jnp.bfloat16)
-    route_weight = jax.nn.softmax(route_logits, axis=-1)
-    combine = combine_matrix(routes, route_weight, capacity)
-    sender = dispatch_matrix(routes, capacity)
-    slot_rows = jnp.einsum(
-        "ecr,rd->ecd", sender, normed, preferred_element_type=jnp.float32
-    ).astype(jnp.bfloat16)
-    messages = slot_rows.reshape(ep_size, -1, 128)
-    returned, attended = layer(messages, gate_weight, up_weight, down_weight, partial_rows)
-    returned = returned.reshape(EXPERTS, capacity, -1)
-    expert_mix = jnp.einsum("rec,ecd->rd", combine, returned.astype(jnp.float32)).astype(
-        jnp.bfloat16
-    )
-    return (attended, expert_mix)
 
 
 def solution(mesh):

time: 127 us -> 110 us (0.87)
  the two profiles are of different devices: /device:TPU:8 before, /device:TPU:4 now
where the time goes in v4:
time: 110 us
  Pallas kernels  107 us (97%)
  local copies, waits for them, and re-layouts  2.26 us (2%)
    pallas_call x1, Pallas kernels, on_device(): pl.pallas_call(layer_kernel, out_shape=(jax.ShapeDtypeStruct((own, width)...  107 us
    unnamed x4, local copies, waits for them, and re-layouts  2.26 us

profile of v4, /device:TPU:4, one launch (start us, length us, event | category | flops | bytes accessed | tf_op | source)
XLA Modules:
  0.0 109.9 jit_solution(6870587688222551083)
XLA Ops:
  0.6 107.0 %layer.1 = (bf16[32,2048]{1,0:T(8,128)(2,1)}, bf16[32,2048]{1,0:T(8,128)(2,1)}) custom-call(bf16[192,512]{1,0:T(8,128)(2,1)} %bitcast.7, bf16[64,512]{1,0:T(8,128)(2,1)} %bitcast.8, bf16[64,512]{1,0:T(8,128)(2,1)} %bitcast.9, f32[3,64]{1,0:T(4,128)} %query_gain_ref.1, f32[1,64]{1,0:T(1,128)} %key_gain_ref.1, f32[1,3]{1,0:T(1,128)} %bitcast.13, ...), custom_call_target="tpu_custom_call" | custom-call | tf_op jit(solution)/shard_map/layer/pallas_call | solution.py:517
  107.6 0.0 copy-start
  107.6 1.6 %copy.18 = bf16[32,2048]{1,0:T(8,128)(2,1)} copy(bf16[32,2048]{1,0:T(8,128)(2,1)} %get-tuple-element.4) | data formatting | bytes 262144
  109.2 0.0 copy-done
  109.2 0.7 copy.19
Async XLA Ops:
  107.6 1.6 %copy-start = (bf16[32,2048]{1,0:T(8,128)(2,1)S(1)}, bf16[32,2048]{1,0:T(8,128)(2,1)}, u32[]{:S(2)}) copy-start(bf16[32,2048]{1,0:T(8,128)(2,1)} %get-tuple-element.5) | copy-start | bytes 393220

commit v5 on v4

--- a/solution.py
+++ b/solution.py
@@ -1,3 +1,5 @@
+import heapq
+
 import jax
 import jax.numpy as jnp
 from jax import lax
@@ -16,7 +18,7 @@
     for _hop in range(1, _far + 1):
         HOPS[_half, _way, _hop] = len(HOPS)
 X_RING = 4
-GROUPS = 2
+GROUPS = 4
 LANES = 128
 VMEM_LIMIT = 60 * 1024 * 1024
 
@@ -59,7 +61,100 @@
     for level in range(1, long // 2):
         for across in (0, 1, X_RING - 1, 2):
             order += [(level, across), (long - level, across)]
-    return order + [(long // 2, across) for across in (0, 1, X_RING - 1, 2)]
+    order += [(long // 2, across) for across in (0, 1, X_RING - 1, 2)]
+    quarter = count // 4
+    return order[:quarter] + order[2 * quarter :] + order[quarter : 2 * quarter]
+
+
+def plan():
+    wire = {"gather": 2.1 * 2 / GROUPS, "sum": 2.1 * 2 / GROUPS, "pair": 1.4}
+    delay = 2.0
+    free = {1: 0.0, -1: 0.0}
+    coming, ready, steps = [], [], []
+    serial = iter(range(1 << 20))
+    done = set()
+    left = {}
+
+    def send(now, kind, group, half, way, hop):
+        free[way] = max(free[way], now) + wire[kind]
+        heapq.heappush(coming, (free[way] + delay, next(serial), (kind, group, half, way, hop)))
+
+    def task(rank, name, cost):
+        heapq.heappush(ready, (rank, next(serial), name, cost))
+
+    for group in range(GROUPS):
+        when = 3.0 + 10.0 * group / (GROUPS - 1)
+        heapq.heappush(coming, (when, next(serial), ("arrive", group)))
+    heapq.heappush(coming, (4.0, next(serial), ("halo",)))
+    for block in (1, 2, 3):
+        task(0, ("attend", block), 1.7)
+    attended = 0
+    now = 0.0
+    blocked = []
+    while coming or ready or blocked:
+        arrived = coming and coming[0][0] <= now
+        if not arrived and ready:
+            rank, _, name, cost = heapq.heappop(ready)
+            steps.append(name)
+            now += cost
+            done.add(name)
+            if name[0] == "attend":
+                attended += 1
+                if attended == 4:
+                    steps.append(("swap",))
+                    heapq.heappush(coming, (now + 3.5, next(serial), ("swapped",)))
+            elif name[0] == "experts":
+                _, group, hop = name
+                for half, way, far in CHAINS:
+                    if hop and far == hop:
+                        steps.append(("start", group, half, way, far))
+                        send(now, "sum", group, half, way, far)
+            for entry in blocked:
+                heapq.heappush(coming, entry)
+            blocked = []
+            continue
+        if not coming:
+            break
+        when, number, event = heapq.heappop(coming)
+        now = max(now, when)
+        if event[0] == "sum":
+            _, group, half, way, hop = event
+            if ("experts", group, hop - 1) not in done:
+                blocked.append((when, number, event))
+                continue
+        steps.append(event)
+        if event[0] == "arrive":
+            now += 0.6
+            for half, way, far in CHAINS:
+                send(now, "gather", event[1], half, way, 1)
+            task(2 + event[1], ("experts", event[1], 0), 0.9)
+        elif event[0] == "halo":
+            task(1, ("attend", 0), 1.7)
+        elif event[0] == "swapped":
+            now += 0.6
+            for half, way, far in CHAINS:
+                send(now, "pair", 0, half, way, far)
+        elif event[0] == "gather":
+            _, group, half, way, hop = event
+            now += 0.05
+            if (half, way, hop + 1) in HOPS:
+                send(now, "gather", group, half, way, hop + 1)
+            key = ("gather", group, hop)
+            left[key] = left.get(key, 0) + 1
+            if left[key] == (4 if hop < 4 else 2):
+                task(2 + group, ("experts", group, hop), 1.6 if hop < 4 else 0.9)
+        else:
+            kind, group, half, way, hop = event
+            now += 0.2
+            if hop > 1:
+                send(now, kind, group, half, way, hop - 1)
+            else:
+                key = (kind, group)
+                left[key] = left.get(key, 0) + 1
+                if left[key] == 4:
+                    steps.append(("finish", kind, group))
+                    now += 0.8
+    return steps
 
 
 def ep_place(me, offset, sign=1):
@@ -199,20 +294,16 @@
             toward(way),
         )
 
-    def running(buffer, received, copy_of, left):
-        for half, way, far in CHAINS:
-            hop = far - 3 + left
-            if hop < 1:
-                continue
-            copy_of(half, way, hop).wait_recv()
-            if hop > 1:
-                slot = (way * (hop - 1)) % ring
-                at = half_columns(half)
-                buffer[slot, :, at] = (
-                    buffer[slot, :, at].astype(jnp.float32)
-                    + received[HOPS[half, way, hop]].astype(jnp.float32)
-                ).astype(jnp.bfloat16)
-                copy_of(half, way, hop - 1).start()
+    def carry_on(buffer, received, copy_of, half, way, hop):
+        copy_of(half, way, hop).wait_recv()
+        if hop > 1:
+            slot = (way * (hop - 1)) % ring
+            at = half_columns(half)
+            buffer[slot, :, at] = (
+                buffer[slot, :, at].astype(jnp.float32)
+                + received[HOPS[half, way, hop]].astype(jnp.float32)
+            ).astype(jnp.bfloat16)
+            copy_of(half, way, hop - 1).start()
 
     def summed(buffer, received, half):
         return (
@@ -247,32 +338,16 @@
         for half, way, far in CHAINS:
             gather_copy(group, half, way, 1).start()
 
-    def gather(group, hop):
-        for half, way, far in CHAINS:
-            if hop <= far:
-                gather_copy(group, half, way, hop).wait_recv()
-                if hop < far:
-                    gather_copy(group, half, way, hop + 1).start()
-        if hop < 4:
-
-            def both(index, carry):
-                experts(group, hop + index * (ring - 2 * hop))
-                return carry
-
-            lax.fori_loop(0, 2, both, 0)
-        else:
-            experts(group, 4)
-        for half, way, far in CHAINS:
-            if far == hop:
-                sum_copy(group, half, way, far).start()
-
-    def collect(group, left):
-        running(
-            pbuf.at[group],
-            rbuf.at[group],
-            lambda half, way, hop: sum_copy(group, half, way, hop),
-            left,
-        )
+    def compute(group, hop):
+        if hop in (0, 4):
+            experts(group, hop)
+            return
+
+        def both(index, carry):
+            experts(group, hop + index * (ring - 2 * hop))
+            return carry
+
+        lax.fori_loop(0, 2, both, 0)
 
     def give_back(group):
         for half in range(2):
@@ -411,56 +486,58 @@
                 .reshape(owners, 2, tokens, step)
             )
 
-    for block in range(1, blocks):
-        attend(block)
-        project(block)
-    for copy in halo:
-        copy.wait_recv()
-    attend(0)
-    project(0)
     swap = remote(part_ref.at[:, 1 - core], swapped, swap_sem.at[0], swap_sem.at[1], partner)
-    swap.start()
-    arrive(0)
-    for copy in local:
-        copy.wait()
-    for copy in shared:
-        copy.wait_recv()
-    experts(0, 0)
-    swap.wait_recv()
-    for slot in (4, 3, 5, 2, 6, 1, 7, 0):
-        owner = lax.rem(spot + slot, ring)
-        pair[slot] = (
-            part_ref[owner, core].astype(jnp.float32) + swapped[owner].astype(jnp.float32)
-        ).astype(jnp.bfloat16)
-        for half, way, far in CHAINS:
-            if (way * far) % ring == slot:
-                pair_copy(half, way, far).start()
-    gather(0, 1)
-    arrive(1)
-    running(pair, prbuf, pair_copy, 3)
-    gather(0, 2)
-    experts(1, 0)
-    running(pair, prbuf, pair_copy, 2)
-    gather(1, 1)
-    gather(0, 3)
-    running(pair, prbuf, pair_copy, 1)
-    gather(1, 2)
-    gather(0, 4)
-    running(pair, prbuf, pair_copy, 0)
-    for half in range(2):
-        attended_ref[:, half_columns(half)] = summed(pair, prbuf, half).astype(jnp.bfloat16)
-    gather(1, 3)
-    collect(0, 3)
-    gather(1, 4)
-    collect(0, 2)
-    collect(1, 3)
-    collect(0, 1)
-    collect(1, 2)
-    collect(0, 0)
-    give_back(0)
-    collect(1, 1)
-    collect(1, 0)
-    give_back(1)
+    weights_wait = [copy.wait for copy in local] + [copy.wait_recv for copy in shared]
+    for name, *rest in plan():
+        if name == "attend":
+            attend(*rest)
+            project(*rest)
+        elif name == "halo":
+            for copy in halo:
+                copy.wait_recv()
+        elif name == "swap":
+            swap.start()
+        elif name == "swapped":
+            swap.wait_recv()
+            for slot in (4, 3, 5, 2, 6, 1, 7, 0):
+                owner = lax.rem(spot + slot, ring)
+                pair[slot] = (
+                    part_ref[owner, core].astype(jnp.float32) + swapped[owner].astype(jnp.float32)
+                ).astype(jnp.bfloat16)
+                for half, way, far in CHAINS:
+                    if (way * far) % ring == slot:
+                        pair_copy(half, way, far).start()
+        elif name == "arrive":
+            arrive(*rest)
+        elif name == "experts":
+            while weights_wait:
+                weights_wait.pop()()
+            compute(*rest)
+        elif name == "start":
+            sum_copy(*rest).start()
+        elif name == "gather":
+            group, half, way, hop = rest
+            gather_copy(group, half, way, hop).wait_recv()
+            if (half, way, hop + 1) in HOPS:
+                gather_copy(group, half, way, hop + 1).start()
+        elif name == "pair":
+            carry_on(pair, prbuf, pair_copy, *rest[1:])
+        elif name == "sum":
+            group = rest[0]
+            carry_on(
+                pbuf.at[group],
+                rbuf.at[group],
+                lambda half, way, hop, group=group: sum_copy(group, half, way, hop),
+                *rest[1:],
+            )
+        elif name == "finish":
+            if rest[0] == "pair":
+                for half in range(2):
+                    attended_ref[:, half_columns(half)] = summed(pair, prbuf, half).astype(
+                        jnp.bfloat16
+                    )
+            else:
+                give_back(rest[1])
     back_ref[me] = sbuf[0]
     swap.wait_send()
     for copy in shared + halo:

time: 110 us -> 109 us (level)
  the two profiles are of different devices: /device:TPU:4 before, /device:TPU:16 now
where the time goes in v5:
time: 109 us
  Pallas kernels  106 us (97%)
  local copies, waits for them, and re-layouts  2.26 us (2%)
    pallas_call x1, Pallas kernels, on_device(): pl.pallas_call(layer_kernel, out_shape=(jax.ShapeDtypeStruct((own, width)...  106 us
    unnamed x4, local copies, waits for them, and re-layouts  2.26 us

profile of v5, /device:TPU:16, one launch (start us, length us, event | category | flops | bytes accessed | tf_op | source)
XLA Modules:
  0.0 108.8 jit_solution(7525420977035997996)
XLA Ops:
  0.6 105.9 %layer.1 = (bf16[32,2048]{1,0:T(8,128)(2,1)}, bf16[32,2048]{1,0:T(8,128)(2,1)}) custom-call(bf16[192,512]{1,0:T(8,128)(2,1)} %bitcast.7, bf16[64,512]{1,0:T(8,128)(2,1)} %bitcast.8, bf16[64,512]{1,0:T(8,128)(2,1)} %bitcast.9, f32[3,64]{1,0:T(4,128)} %query_gain_ref.1, f32[1,64]{1,0:T(1,128)} %key_gain_ref.1, f32[1,3]{1,0:T(1,128)} %bitcast.13, ...), custom_call_target="tpu_custom_call" | custom-call | tf_op jit(solution)/shard_map/layer/pallas_call | solution.py:594
  106.5 0.0 copy-start
  106.5 1.6 %copy.18 = bf16[32,2048]{1,0:T(8,128)(2,1)} copy(bf16[32,2048]{1,0:T(8,128)(2,1)} %get-tuple-element.4) | data formatting | bytes 262144
  108.1 0.0 copy-done
  108.1 0.7 copy.19
Async XLA Ops:
  106.5 1.6 %copy-start = (bf16[32,2048]{1,0:T(8,128)(2,1)S(1)}, bf16[32,2048]{1,0:T(8,128)(2,1)}, u32[]{:S(2)}) copy-start(bf16[32,2048]{1,0:T(8,128)(2,1)} %get-tuple-element.5) | copy-start | bytes 393220

commit v6 on v5

--- a/solution.py
+++ b/solution.py
@@ -20,6 +20,8 @@
 X_RING = 4
 GROUPS = 4
 LANES = 128
+FAR = 1024
+PAD = 32
 VMEM_LIMIT = 60 * 1024 * 1024
 
 
@@ -67,7 +69,15 @@
 
 
 def plan():
-    wire = {"gather": 2.1 * 2 / GROUPS, "sum": 2.1 * 2 / GROUPS, "pair": 1.4}
+    low = 1.0 - FAR / 2048
+    wire = {
+        "gather": 2.25 * 2 / GROUPS,
+        "sum": 2.25 * 2 / GROUPS * low,
+        "pair": 1.5,
+        "home": 1.5 * (1.0 - low),
+    }
+    plane = 13.0
+    arrived_far = 0
     delay = 2.0
     free = {1: 0.0, -1: 0.0}
     coming, ready, steps = [], [], []
@@ -86,6 +96,7 @@
         when = 3.0 + 10.0 * group / (GROUPS - 1)
         heapq.heappush(coming, (when, next(serial), ("arrive", group)))
     heapq.heappush(coming, (4.0, next(serial), ("halo",)))
+    heapq.heappush(coming, (7.0, next(serial), ("tables",)))
     for block in (1, 2, 3):
         task(0, ("attend", block), 1.7)
     attended = 0
@@ -105,10 +116,19 @@
                     heapq.heappush(coming, (now + 3.5, next(serial), ("swapped",)))
             elif name[0] == "experts":
                 _, group, hop = name
+                left[group] = left.get(group, 0) + 1
+                if left[group] == 5:
+                    steps.append(("send_far", group))
+                    now += 0.5
+                    plane = max(plane, now) + 69.0 / GROUPS * (1.0 - low)
+                    heapq.heappush(coming, (plane + 4.0, next(serial), ("far", group)))
                 for half, way, far in CHAINS:
                     if hop and far == hop:
                         steps.append(("start", group, half, way, far))
                         send(now, "sum", group, half, way, far)
+            elif name[0] == "relay":
+                for half, way, far in CHAINS:
+                    send(now, "home", 0, half, way, far)
             for entry in blocked:
                 heapq.heappush(coming, entry)
             blocked = []
@@ -130,6 +150,12 @@
             task(2 + event[1], ("experts", event[1], 0), 0.9)
         elif event[0] == "halo":
             task(1, ("attend", 0), 1.7)
+        elif event[0] == "tables":
+            now += 1.0
+        elif event[0] == "far":
+            arrived_far += 1
+            if arrived_far == GROUPS:
+                task(1, ("relay",), 3.0)
         elif event[0] == "swapped":
             now += 0.6
             for half, way, far in CHAINS:
@@ -217,6 +243,20 @@
     pr_sem,
     hs_sem,
     hr_sem,
+    wide,
+    fsend,
+    fbuf,
+    tables,
+    coarse_all,
+    fine_all,
+    mixed_part,
+    qbuf,
+    fs_sem,
+    fr_sem,
+    ts_sem,
+    tr_sem,
+    qs_sem,
+    qr_sem,
 ):
     me = lax.axis_index("ep")
     count = lax.axis_size("ep")
@@ -231,6 +271,11 @@
     members = count // GROUPS
     rows, width = xbuf.shape[2], xbuf.shape[3]
     strip = width // LANES
+    low = width - FAR
+    low_strip = low // LANES
+
+    def around(step):
+        return {"tp": lax.rem(spot + step, ring) * 2 + core}
 
     local = [
         pltpu.make_async_copy(gate_ref.at[0], w1.at[:, pl.ds(0, inner)], wl_sem.at[0]),
@@ -239,7 +284,8 @@
     ]
     for copy in local:
         copy.start()
-    peers = [ahead, behind, partner] + [{"ep": ep_place(me, offset)} for offset in order[1:]]
+    peers = [around(step) for step in range(1, ring)] + [partner]
+    peers += [{"ep": ep_place(me, offset)} for offset in order[1:]]
     barrier = pltpu.get_barrier_semaphore()
     for place in peers:
         pl.semaphore_signal(
@@ -260,6 +306,9 @@
 
     def half_columns(half):
         return pl.ds(half * (width // 2), width // 2)
+
+    def low_columns(half):
+        return pl.ds(half * (low // 2), low // 2)
 
     def toward(way):
         return ahead if way == 1 else behind
@@ -277,7 +326,7 @@
     def sum_copy(group, half, way, hop):
         number = HOPS[half, way, hop]
         return remote(
-            pbuf.at[group, (way * hop) % ring, :, half_columns(half)],
+            pbuf.at[group, (way * hop) % ring, :, low_columns(half)],
             rbuf.at[group, number],
             ss_sem.at[group, number],
             sr_sem.at[group, number],
@@ -294,20 +343,51 @@
             toward(way),
         )
 
-    def carry_on(buffer, received, copy_of, half, way, hop):
+    def far_copy(number):
+        peer = ep_place(me, order[number], -1)
+        return remote(
+            fsend.at[number],
+            fbuf.at[me, pl.ds(0, fsend.shape[1])],
+            fs_sem.at[number],
+            fr_sem.at[number],
+            {"ep": peer},
+        )
+
+    def home_copy(half, way, hop):
+        number = HOPS[half, way, hop]
+        at = pl.ds(half * (FAR // 2), FAR // 2)
+        return remote(
+            mixed_part.at[lax.rem(spot + (way * hop) % ring, ring), :, at],
+            qbuf.at[number],
+            qs_sem.at[number],
+            qr_sem.at[number],
+            toward(way),
+        )
+
+    def table_copy(step):
+        return remote(
+            tables.at[0], tables.at[step], ts_sem.at[step], tr_sem.at[step], around(step)
+        )
+
+    def carry_on(buffer, received, copy_of, columns, half, way, hop):
         copy_of(half, way, hop).wait_recv()
         if hop > 1:
             slot = (way * (hop - 1)) % ring
-            at = half_columns(half)
+            if columns is home_columns:
+                slot = lax.rem(spot + slot, ring)
+            at = columns(half)
             buffer[slot, :, at] = (
                 buffer[slot, :, at].astype(jnp.float32)
                 + received[HOPS[half, way, hop]].astype(jnp.float32)
             ).astype(jnp.bfloat16)
             copy_of(half, way, hop - 1).start()
 
-    def summed(buffer, received, half):
+    def home_columns(half):
+        return pl.ds(half * (FAR // 2), FAR // 2)
+
+    def summed(buffer, received, columns, half, own=0):
         return (
-            buffer[0, :, half_columns(half)].astype(jnp.float32)
+            buffer[own, :, columns(half)].astype(jnp.float32)
             + received[HOPS[half, 1, 1]].astype(jnp.float32)
             + received[HOPS[half, -1, 1]].astype(jnp.float32)
         )
@@ -351,17 +431,72 @@
 
     def give_back(group):
         for half in range(2):
-            total = summed(pbuf.at[group], rbuf.at[group], half)
-            for at in range(strip // 2):
-                turn[pl.ds(half * (strip // 2) + at, rows, stride=strip), :] = total[
+            total = summed(pbuf.at[group], rbuf.at[group], low_columns, half)
+            for at in range(low_strip // 2):
+                turn[pl.ds(half * (low_strip // 2) + at, rows, stride=low_strip), :] = total[
                     :, at * LANES : (at + 1) * LANES
                 ]
         sbuf[group * members : (group + 1) * members] = (
-            turn[: rows * strip].reshape(members, -1, LANES).astype(jnp.bfloat16)
+            turn[: rows * low_strip].reshape(members, -1, LANES).astype(jnp.bfloat16)
         )
         for number in range(group * members, (group + 1) * members):
             if number > 0:
                 back_copy(number).start()
+
+    def send_far(group):
+        for slot in range(ring):
+            for at in range(FAR // LANES):
+                wide[at, slot * rows : (slot + 1) * rows, :] = pbuf[
+                    group, slot, :, low + at * LANES : low + (at + 1) * LANES
+                ].astype(jnp.float32)
+        for member in range(members):
+            number = group * members + member
+            for at in range(FAR // LANES):
+                fsend[number, :, at * LANES : (at + 1) * LANES] = jnp.concatenate(
+                    [
+                        wide[at, pl.ds(member * capacity + place, ring, stride=rows), :]
+                        for place in range(capacity)
+                    ],
+                    axis=0,
+                ).astype(jnp.bfloat16)
+            if number > 0:
+                far_copy(number).start()
+        if group == 0:
+            fbuf[me, : fsend.shape[1]] = fsend[0]
+
+    def relay():
+        everything = fbuf[...].reshape(count * PAD, FAR)
+        for at in range(0, FAR, 256):
+            part = everything[:, at : at + 256]
+            mixed_part[:, :, at : at + 256] = (
+                (contract_rows(coarse_all[...], part) + contract_rows(fine_all[...], part))
+                .astype(jnp.bfloat16)
+                .reshape(ring, tokens, 256)
+            )
+
+    def spread_tables():
+        table = tables[0]
+        for step in range(1, ring):
+            table_copy(step).wait_recv()
+            table = table + tables[step]
+        lane = lax.broadcasted_iota(jnp.int32, (1, ring * tokens), 1)
+        turned = lax.rem(lax.div(lane, tokens) + ring - spot, ring).astype(jnp.float32)
+        block = 256
+        for at in range(0, count * PAD, block):
+            spot_row = lax.broadcasted_iota(jnp.int32, (block, ring * tokens), 0).astype(
+                jnp.float32
+            ) + float(at)
+            total = jnp.zeros((block, ring * tokens), jnp.float32)
+            for copy in range(2):
+                target = (
+                    float(PAD) * table[copy : copy + 1]
+                    + float(ring) * table[2 + copy : 3 + copy]
+                    + turned
+                )
+                total += jnp.where(spot_row == target, table[4 + copy : 5 + copy], 0.0)
+            rounded = total.astype(jnp.bfloat16)
+            coarse_all[at : at + block] = rounded
+            fine_all[at : at + block] = (total - rounded.astype(jnp.float32)).astype(jnp.bfloat16)
 
     head_size = key_ref.shape[0]
     group_heads = query_ref.shape[0] // head_size
@@ -405,10 +540,24 @@
     coarse = weighted.astype(jnp.bfloat16)
     fine = (weighted - coarse.astype(jnp.float32)).astype(jnp.bfloat16)
     sender = (picked[0] + picked[1]).astype(jnp.bfloat16)
-    step = width // 4
-    for at in range(0, width, step):
-        slot_rows = jnp.dot(sender, normed[:, at : at + step], preferred_element_type=jnp.float32)
-        for lane in range(0, step, LANES):
+    earlier = [
+        jnp.sum(jnp.where(gap == 0, taken, 0.0), axis=0, keepdims=True) for gap in offset
+    ]
+    lines = [routes_ref[copy : copy + 1, :].astype(jnp.float32) for copy in range(2)]
+    lines += earlier + [share[0:1, :], share[1:2, :]]
+    line = lax.broadcasted_iota(jnp.int32, (8, tokens), 0)
+    own_table = jnp.zeros((8, tokens), jnp.float32)
+    for index, values_line in enumerate(lines):
+        own_table = jnp.where(line == index, values_line, own_table)
+    lane_owner = lax.div(lax.broadcasted_iota(jnp.int32, (8, ring * tokens), 1), tokens)
+    tables[0] = jnp.where(lane_owner == spot, jnp.concatenate([own_table] * ring, axis=1), 0.0)
+    fbuf[:, fsend.shape[1] :, :] = jnp.zeros(
+        (count, PAD - fsend.shape[1], FAR), jnp.bfloat16
+    )
+    stride = width // 4
+    for at in range(0, width, stride):
+        slot_rows = jnp.dot(sender, normed[:, at : at + stride], preferred_element_type=jnp.float32)
+        for lane in range(0, stride, LANES):
             turn[pl.ds((at + lane) // LANES, slots, stride=strip), :] = slot_rows[
                 :, lane : lane + LANES
             ]
@@ -428,6 +577,8 @@
     ]
     for copy in halo:
         copy.start()
+    for step in range(1, ring):
+        table_copy(step).start()
     for number in range(1, count):
         out_copy(number).start()
     shared = [
@@ -479,11 +630,11 @@
     def project(block):
         owners = WINDOW // tokens // 2
         rows_in = heads[:, block * WINDOW : (block + 1) * WINDOW]
-        for at in range(0, width, step):
-            part_ref[block * owners : (block + 1) * owners, :, :, at : at + step] = (
-                contract_rows(rows_in, project_ref[:, at : at + step])
+        for at in range(0, width, stride):
+            part_ref[block * owners : (block + 1) * owners, :, :, at : at + stride] = (
+                contract_rows(rows_in, project_ref[:, at : at + stride])
                 .astype(jnp.bfloat16)
-                .reshape(owners, 2, tokens, step)
+                .reshape(owners, 2, tokens, stride)
             )
 
     swap = remote(part_ref.at[:, 1 - core], swapped, swap_sem.at[0], swap_sem.at[1], partner)
@@ -521,19 +672,40 @@
             if (half, way, hop + 1) in HOPS:
                 gather_copy(group, half, way, hop + 1).start()
         elif name == "pair":
-            carry_on(pair, prbuf, pair_copy, *rest[1:])
+            carry_on(pair, prbuf, pair_copy, half_columns, *rest[1:])
+        elif name == "home":
+            carry_on(mixed_part, qbuf, home_copy, home_columns, *rest[1:])
+        elif name == "tables":
+            spread_tables()
+        elif name == "send_far":
+            send_far(*rest)
+        elif name == "far":
+            for number in range(rest[0] * members, (rest[0] + 1) * members):
+                if number > 0:
+                    far_copy(number).wait_recv()
+        elif name == "relay":
+            relay()
+            for half, way, far in CHAINS:
+                home_copy(half, way, far).start()
         elif name == "sum":
             group = rest[0]
             carry_on(
                 pbuf.at[group],
                 rbuf.at[group],
                 lambda half, way, hop, group=group: sum_copy(group, half, way, hop),
+                low_columns,
                 *rest[1:],
             )
         elif name == "finish":
             if rest[0] == "pair":
                 for half in range(2):
-                    attended_ref[:, half_columns(half)] = summed(pair, prbuf, half).astype(
+                    attended_ref[:, half_columns(half)] = summed(
+                        pair, prbuf, half_columns, half
+                    ).astype(jnp.bfloat16)
+            elif rest[0] == "home":
+                for half in range(2):
+                    at = pl.ds(low + half * (FAR // 2), FAR // 2)
+                    mix_ref[:, at] = summed(mixed_part, qbuf, home_columns, half, spot).astype(
                         jnp.bfloat16
                     )
             else:
@@ -544,15 +716,19 @@
         copy.wait_send()
     for half, way, hop in HOPS:
         pair_copy(half, way, hop).wait_send()
+        home_copy(half, way, hop).wait_send()
         for group in range(GROUPS):
             gather_copy(group, half, way, hop).wait_send()
             sum_copy(group, half, way, hop).wait_send()
     for number in range(1, count):
         out_copy(number).wait_send()
+        far_copy(number).wait_send()
         back_copy(number).wait()
-    turn[...] = back_ref[...].astype(jnp.float32).reshape(turn.shape)
-    for at in range(strip):
-        came = turn[pl.ds(at, slots, stride=strip), :].astype(jnp.bfloat16)
+    for step in range(1, ring):
+        table_copy(step).wait_send()
+    turn[: slots * low_strip] = back_ref[...].astype(jnp.float32).reshape(-1, LANES)
+    for at in range(low_strip):
+        came = turn[pl.ds(at, slots, stride=low_strip), :].astype(jnp.bfloat16)
         mix_ref[:, at * LANES : (at + 1) * LANES] = (
             contract_rows(coarse, came) + contract_rows(fine, came)
         ).astype(jnp.bfloat16)
@@ -584,6 +760,7 @@
     seq_rows, query_width = query_rows.shape
     head_size = key_rows.shape[1]
     message = (count, capacity * width // LANES, LANES)
+    low_message = (count, capacity * (width - FAR) // LANES, LANES)
     hops = len(HOPS)
     dma = pltpu.SemaphoreType.DMA
     vmem = pl.BlockSpec(memory_space=pltpu.VMEM)
@@ -601,7 +778,7 @@
         out_specs=[vmem] * 2,
         scratch_shapes=[
             scratch(*message),
-            scratch(*message),
+            scratch(*low_message),
             scratch(head_size, seq_rows + WINDOW),
             scratch(head_size, seq_rows + WINDOW),
             scratch(seq_rows // WINDOW, head_size, query_width // head_size * WINDOW),
@@ -613,8 +790,8 @@
             pltpu.VMEM((count * capacity * width // LANES, LANES), jnp.float32),
             scratch(GROUPS, ring, rows, width),
             scratch(GROUPS, ring, rows, width),
-            scratch(GROUPS, hops, rows, width // 2),
-            scratch(*message),
+            scratch(GROUPS, hops, rows, (width - FAR) // 2),
+            scratch(*low_message),
             scratch(ring, own, width),
             scratch(ring, own, width),
             scratch(hops, own, width // 2),
@@ -634,6 +811,20 @@
             dma((hops,)),
             dma((2,)),
             dma((2,)),
+            pltpu.VMEM((FAR // LANES, ring * rows, LANES), jnp.float32),
+            scratch(count, ring * capacity, FAR),
+            scratch(count, PAD, FAR),
+            pltpu.VMEM((ring, 8, ring * own), jnp.float32),
+            scratch(count * PAD, ring * own),
+            scratch(count * PAD, ring * own),
+            scratch(ring, own, FAR),
+            scratch(hops, own, FAR // 2),
+            dma((count,)),
+            dma((count,)),
+            dma((ring,)),
+            dma((ring,)),
+            dma((hops,)),
+            dma((hops,)),
         ],
         compiler_params=pltpu.CompilerParams(
             collective_id=1, has_side_effects=True, vmem_limit_bytes=VMEM_LIMIT

time: 109 us -> 118 us (1.083)
  the two profiles are of different devices: /device:TPU:16 before, /device:TPU:14 now
where the time goes in v6:
time: 118 us
  Pallas kernels  115 us (97%)
  local copies, waits for them, and re-layouts  2.26 us (2%)
    pallas_call x1, Pallas kernels, on_device(): pl.pallas_call(layer_kernel, out_shape=(jax.ShapeDtypeStruct((own, width)...  115 us

profile of v6, /device:TPU:14, one launch (start us, length us, event | category | flops | bytes accessed | tf_op | source)
XLA Modules:
  0.0 118.2 jit_solution(16107963915816170621)
XLA Ops:
  0.6 115.3 %layer.1 = (bf16[32,2048]{1,0:T(8,128)(2,1)}, bf16[32,2048]{1,0:T(8,128)(2,1)}) custom-call(bf16[192,512]{1,0:T(8,128)(2,1)} %bitcast.7, bf16[64,512]{1,0:T(8,128)(2,1)} %bitcast.8, bf16[64,512]{1,0:T(8,128)(2,1)} %bitcast.9, f32[3,64]{1,0:T(4,128)} %query_gain_ref.1, f32[1,64]{1,0:T(1,128)} %key_gain_ref.1, f32[1,3]{1,0:T(1,128)} %bitcast.13, ...), custom_call_target="tpu_custom_call" | custom-call | tf_op jit(solution)/shard_map/layer/pallas_call | solution.py:771
  116.0 0.0 copy-start
  116.0 1.6 %copy.18 = bf16[32,2048]{1,0:T(8,128)(2,1)} copy(bf16[32,2048]{1,0:T(8,128)(2,1)} %get-tuple-element.4) | data formatting | bytes 262144
  117.6 0.0 copy-done
  117.6 0.7 copy.19
Async XLA Ops:
  116.0 1.6 %copy-start = (bf16[32,2048]{1,0:T(8,128)(2,1)S(1)}, bf16[32,2048]{1,0:T(8,128)(2,1)}, u32[]{:S(2)}) copy-start(bf16[32,2048]{1,0:T(8,128)(2,1)} %get-tuple-element.5) | copy-start | bytes 393220

commit v7 on v6

--- a/solution.py
+++ b/solution.py
@@ -20,7 +20,7 @@
 X_RING = 4
 GROUPS = 4
 LANES = 128
-FAR = 1024
+FAR = 512
 PAD = 32
 VMEM_LIMIT = 60 * 1024 * 1024
 

time: 118 us -> 104 us (0.88)
  the two profiles are of different devices: /device:TPU:14 before, /device:TPU:24 now
where the time goes in v7:
time: 104 us; the launch traced here: 103 us
  Pallas kernels  100 us (96%)
  local copies, waits for them, and re-layouts  2.26 us (2%)
    pallas_call x1, Pallas kernels, on_device(): pl.pallas_call(layer_kernel, out_shape=(jax.ShapeDtypeStruct((own, width)...  100 us
    unnamed x4, local copies, waits for them, and re-layouts  2.26 us

profile of v7, /device:TPU:24, one launch (start us, length us, event | category | flops | bytes accessed | tf_op | source)
XLA Modules:
  0.0 103.4 jit_solution(9102558412274767740)
XLA Ops:
  0.6 100.4 %layer.1 = (bf16[32,2048]{1,0:T(8,128)(2,1)}, bf16[32,2048]{1,0:T(8,128)(2,1)}) custom-call(bf16[192,512]{1,0:T(8,128)(2,1)} %bitcast.7, bf16[64,512]{1,0:T(8,128)(2,1)} %bitcast.8, bf16[64,512]{1,0:T(8,128)(2,1)} %bitcast.9, f32[3,64]{1,0:T(4,128)} %query_gain_ref.1, f32[1,64]{1,0:T(1,128)} %key_gain_ref.1, f32[1,3]{1,0:T(1,128)} %bitcast.13, ...), custom_call_target="tpu_custom_call" | custom-call | tf_op jit(solution)/shard_map/layer/pallas_call | solution.py:771
  101.1 0.0 copy-start
  101.1 1.6 %copy.18 = bf16[32,2048]{1,0:T(8,128)(2,1)} copy(bf16[32,2048]{1,0:T(8,128)(2,1)} %get-tuple-element.4) | data formatting | bytes 262144
  102.7 0.0 copy-done
  102.7 0.7 copy.19
Async XLA Ops:
  101.1 1.6 %copy-start = (bf16[32,2048]{1,0:T(8,128)(2,1)S(1)}, bf16[32,2048]{1,0:T(8,128)(2,1)}, u32[]{:S(2)}) copy-start(bf16[32,2048]{1,0:T(8,128)(2,1)} %get-tuple-element.5) | copy-start | bytes 393220

commit v8 on v7

--- a/solution.py
+++ b/solution.py
@@ -65,7 +65,7 @@
             order += [(level, across), (long - level, across)]
     order += [(long // 2, across) for across in (0, 1, X_RING - 1, 2)]
     quarter = count // 4
-    return order[:quarter] + order[2 * quarter :] + order[quarter : 2 * quarter]
+    return order[: 2 * quarter] + order[3 * quarter :] + order[2 * quarter : 3 * quarter]
 
 
 def plan():
@@ -727,9 +727,12 @@
     for step in range(1, ring):
         table_copy(step).wait_send()
     turn[: slots * low_strip] = back_ref[...].astype(jnp.float32).reshape(-1, LANES)
-    for at in range(low_strip):
-        came = turn[pl.ds(at, slots, stride=low_strip), :].astype(jnp.bfloat16)
-        mix_ref[:, at * LANES : (at + 1) * LANES] = (
+    for at in range(0, low_strip, 4):
+        came = jnp.concatenate(
+            [turn[pl.ds(at + i, slots, stride=low_strip), :].astype(jnp.bfloat16) for i in range(4)],
+            axis=1,
+        )
+        mix_ref[:, at * LANES : (at + 4) * LANES] = (
             contract_rows(coarse, came) + contract_rows(fine, came)
         ).astype(jnp.bfloat16)
 

time: 104 us -> 103 us (level)
  the two profiles are of different devices: /device:TPU:24 before, /device:TPU:16 now
where the time goes in v8:
time: 103 us
  Pallas kernels  100 us (97%)
  local copies, waits for them, and re-layouts  2.26 us (2%)
    pallas_call x1, Pallas kernels, on_device(): pl.pallas_call(layer_kernel, out_shape=(jax.ShapeDtypeStruct((own, width)...  100 us
    unnamed x4, local copies, waits for them, and re-layouts  2.26 us

profile of v8, /device:TPU:16, one launch (start us, length us, event | category | flops | bytes accessed | tf_op | source)
XLA Modules:
  0.0 103.1 jit_solution(9881702111054051841)
XLA Ops:
  0.6 100.2 %layer.1 = (bf16[32,2048]{1,0:T(8,128)(2,1)}, bf16[32,2048]{1,0:T(8,128)(2,1)}) custom-call(bf16[192,512]{1,0:T(8,128)(2,1)} %bitcast.7, bf16[64,512]{1,0:T(8,128)(2,1)} %bitcast.8, bf16[64,512]{1,0:T(8,128)(2,1)} %bitcast.9, f32[3,64]{1,0:T(4,128)} %query_gain_ref.1, f32[1,64]{1,0:T(1,128)} %key_gain_ref.1, f32[1,3]{1,0:T(1,128)} %bitcast.13, ...), custom_call_target="tpu_custom_call" | custom-call | tf_op jit(solution)/shard_map/layer/pallas_call | solution.py:774
  100.8 0.0 copy-start
  100.8 1.6 %copy.18 = bf16[32,2048]{1,0:T(8,128)(2,1)} copy(bf16[32,2048]{1,0:T(8,128)(2,1)} %get-tuple-element.4) | data formatting | bytes 262144
  102.4 0.0 copy-done
  102.4 0.7 copy.19
Async XLA Ops:
  100.8 1.6 %copy-start = (bf16[32,2048]{1,0:T(8,128)(2,1)S(1)}, bf16[32,2048]{1,0:T(8,128)(2,1)}, u32[]{:S(2)}) copy-start(bf16[32,2048]{1,0:T(8,128)(2,1)} %get-tuple-element.5) | copy-start | bytes 393220
